TPU v7x, 256 devices: a whole 4x4x8 slice. The times are simulated.
256 devices in a mesh: ep: 32 (over z, x), tp: 8 (over y, core).
Axes of the slice: x: 4, y: 4, z: 8, core: 2. Of those that a mesh axis runs over, the one named last changes fastest.
Arguments:
- hidden: bfloat16 [1024, 4096], P('ep', 'tp'), may hold values from -6 to 6
- norm_gain: float32 [4096], P('tp'), may hold values from 0.1 to 1.9
- expert_ids: int32 [1024, 8], P('ep'), may hold values from 0 to 63, as said below
- route_weights: float32 [1024, 8], P('ep'), may hold values from 0.1 to 1
- lengths: int32 [128], P('ep'), may hold values from 1 to 8, as said below
- gate_proj: bfloat16 [64, 4096, 1024], P('ep', None, 'tp'), may hold values from -0.09375 to 0.09375
- up_proj: bfloat16 [64, 4096, 1024], P('ep', None, 'tp'), may hold values from -0.09375 to 0.09375
- down_proj: bfloat16 [64, 1024, 4096], P('ep', 'tp'), may hold values from -0.1875 to 0.1875
- shared_gate: bfloat16 [4096, 1024], P(None, 'tp'), may hold values from -0.09375 to 0.09375
- shared_up: bfloat16 [4096, 1024], P(None, 'tp'), may hold values from -0.09375 to 0.09375
- shared_down: bfloat16 [1024, 4096], P('tp'), may hold values from -0.1875 to 0.1875
Outputs:
- mixed: bfloat16 [1024, 4096], P('ep', 'tp')
Inputs may be any that keep to these rules, and one draw needn't show every extreme that they name: `expert_ids`: among the 32 rows of one index of ep (an aligned block), no expert is named more than 12 times, and in every block one expert is named exactly 12 times; each row names 8 different experts. `lengths`: each sequence has 1 to 8 live slots; on some index of ep all 4 sequences have 8 live slots.
All inputs are finite; a program needn't handle non-finite values.
Results may differ from a plain program's by a relative error of at most 0.015.
Values may be sent and summed in bfloat16 or wider, within the bound.
A program may use at most 128 MiB of HBM per device.

v0:
```python
import jax
import jax.numpy as jnp
from jax import lax
from jax.sharding import PartitionSpec as P

epsilon = 1e-06


def in_order(tiles, dim):
    lengths = list(tiles.shape[1:])
    lengths[dim] *= tiles.shape[0]
    return jnp.moveaxis(tiles, 0, dim).reshape(lengths)


def sent_to_all(value, axis):
    size = lax.axis_size(axis)
    return lax.all_to_all(
        jnp.broadcast_to(value[None], (size, *value.shape)), axis, 0, 0, tiled=True
    )


def gathered_copies(value, axis, dim):
    return in_order(sent_to_all(value, axis), dim)


def over_copies(value, axis):
    everything = sent_to_all(value, axis)
    return jnp.sum(everything, axis=0)


def cut_along(value, dim, size):
    before, after = (value.shape[:dim], value.shape[dim + 1 :])
    return jnp.moveaxis(value.reshape(*before, size, -1, *after), dim, 0)


def summed_on_arrival(value, axis, dim):
    tiles = cut_along(value, dim, lax.axis_size(axis))
    arrived = lax.all_to_all(tiles, axis, split_axis=0, concat_axis=0, tiled=True)
    return arrived.astype(jnp.float32).sum(axis=0)


def expert_inner(arrived, gate_proj, up_proj):
    gate_value = jnp.einsum(
        "gecd,edf->gecf", arrived, gate_proj, preferred_element_type=jnp.float32
    )
    up_value = jnp.einsum("gecd,edf->gecf", arrived, up_proj, preferred_element_type=jnp.float32)
    return (jax.nn.silu(gate_value) * up_value).astype(jnp.bfloat16)


def widen_rows(arrived):
    flat_rows = arrived.reshape(-1, arrived.shape[-1])
    widened = gathered_copies(flat_rows, "tp", 1)
    return widened.reshape(arrived.shape[:-1] + (widened.shape[1],))


def dispatch_plan(source_rows, expert_ids, is_live, expert_count, capacity, local_experts):
    slot_count, top_count = expert_ids.shape
    flat_ids = expert_ids.reshape(-1)
    flat_live = jnp.repeat(is_live, top_count)
    hit_matrix = (
        (flat_ids[:, None] == jnp.arange(expert_count, dtype=jnp.int32)[None, :])
        & flat_live[:, None]
    ).astype(jnp.int32)
    earlier = jnp.cumsum(hit_matrix, axis=0) - hit_matrix
    position = jnp.sum(hit_matrix * earlier, axis=1)
    total_slots = expert_count * capacity
    slot_index = jnp.where(flat_live, flat_ids * capacity + position, total_slots)
    chooser = jnp.any(
        slot_index.reshape(slot_count, top_count)[None, :, :]
        == jnp.arange(total_slots, dtype=jnp.int32)[:, None, None],
        axis=2,
    )
    outgoing = jnp.dot(
        chooser.astype(jnp.bfloat16), source_rows, preferred_element_type=jnp.float32
    ).astype(jnp.bfloat16)
    outgoing = outgoing.reshape(lax.axis_size("ep"), local_experts, capacity, source_rows.shape[1])
    return (outgoing, slot_index)


def collect_rows(returned, slot_index, mixing):
    slot_count, top_count = mixing.shape
    back_flat = returned.reshape(-1, returned.shape[3])
    total_slots = back_flat.shape[0]
    picked = jnp.take(back_flat, jnp.minimum(slot_index, total_slots - 1), axis=0)
    picked = picked.reshape(slot_count, top_count, back_flat.shape[1])
    return jnp.sum(mixing[:, :, None] * picked, axis=1)


def body(
    hidden,
    norm_gain,
    expert_ids,
    route_weights,
    lengths,
    gate_proj,
    up_proj,
    down_proj,
    shared_gate,
    shared_up,
    shared_down,
):
    slot_count = hidden.shape[0]
    top_count = expert_ids.shape[1]
    span_size = slot_count // lengths.shape[0]
    local_experts = gate_proj.shape[0]
    expert_count = local_experts * lax.axis_size("ep")
    capacity = min(
        slot_count, max(2, (3 * slot_count * top_count + expert_count - 1) // expert_count)
    )
    model_width = hidden.shape[1] * lax.axis_size("tp")
    values = hidden.astype(jnp.float32)
    squares = over_copies(jnp.sum(values * values, axis=1), "tp")
    row_scale = lax.rsqrt(squares / model_width + epsilon)
    normed = (values * row_scale[:, None] * norm_gain[None, :]).astype(jnp.bfloat16)
    full_rows = gathered_copies(normed, "tp", 1)
    offsets = jnp.arange(slot_count, dtype=jnp.int32) % span_size
    is_live = offsets < jnp.repeat(lengths, span_size)
    mixing = jnp.where(is_live[:, None], route_weights, 0.0)
    shared_inner = (
        jax.nn.silu(jnp.dot(full_rows, shared_gate, preferred_element_type=jnp.float32))
        * jnp.dot(full_rows, shared_up, preferred_element_type=jnp.float32)
    ).astype(jnp.bfloat16)
    shared_part = jnp.dot(shared_inner, shared_down, preferred_element_type=jnp.float32)
    outgoing, slot_index = dispatch_plan(
        normed, expert_ids, is_live, expert_count, capacity, local_experts
    )
    down_share = lax.all_to_all(down_proj, "tp", split_axis=2, concat_axis=1, tiled=True)
    inner_value = expert_inner(
        widen_rows(lax.all_to_all(outgoing, "ep", split_axis=0, concat_axis=0, tiled=True)),
        gate_proj,
        up_proj,
    )
    inner_whole = gathered_copies(inner_value, "tp", 3)
    result = jnp.einsum(
        "gecf,efd->gecd", inner_whole, down_share, preferred_element_type=jnp.float32
    )
    returned = lax.all_to_all(
        result.astype(jnp.bfloat16), "ep", split_axis=0, concat_axis=0, tiled=True
    ).astype(result.dtype)
    routed = collect_rows(returned, slot_index, mixing)
    combined = routed + summed_on_arrival(shared_part.astype(jnp.bfloat16), "tp", 1)
    return jnp.where(is_live[:, None], combined, 0.0).astype(jnp.bfloat16)


def solution(mesh):
    placed = (
        P("ep", "tp"),
        P("tp"),
        P("ep", None),
        P("ep", None),
        P("ep"),
        P("ep", None, "tp"),
        P("ep", None, "tp"),
        P("ep", "tp", None),
        P(None, "tp"),
        P(None, "tp"),
        P("tp", None),
    )
    return jax.shard_map(body, mesh=mesh, in_specs=placed, out_specs=P("ep", "tp"), check_vma=False)
```

profile of v0, /device:TPU:1, one launch (start us, length us, event | category | flops | bytes accessed | tf_op | source)
XLA Modules:
  0.0 255.1 jit_solution(8316562800688118385)
XLA Ops:
  1.6 6.4 %all-to-all-start = ((f32[8,1,32]{2,1,0:T(1,128)}), f32[8,1,32]{2,1,0:T(1,128)S(1)}, u32[]{:S(2)}, u32[]{:S(2)}) async-start(f32[8,1,32]{2,1,0:T(1,128)} %broadcast_in_dim.97), calls=%async_computation | async-start | bytes 8192 | tf_op jit(solution)/shard_map/all_to_all | solution.py:17
  16.8 31.5 %all_to_all.54 = bf16[32,2,12,512]{3,1,2,0:T(2,128)(2,1)} all-to-all(bf16[32,2,12,512]{3,1,2,0:T(2,128)(2,1)S(1)} %copy.99), channel_id=1, replica_groups=mesh['ep'=32,'tp'=8] {'ep'}, dimensions={0} | all-to-all | bytes 1572864 | tf_op jit(solution)/shard_map/all_to_all | solution.py:129
  49.1 7.4 %all-to-all-start.6 = ((bf16[8,32,512]{2,1,0:T(8,128)(2,1)}), bf16[8,32,512]{2,1,0:T(8,128)(2,1)S(1)}, u32[]{:S(2)}, u32[]{:S(2)}) async-start(bf16[8,32,512]{2,1,0:T(8,128)(2,1)} %broadcast_in_dim.103), calls=%async_computation.6 | async-start | bytes 524288 | tf_op jit(solution)/shard_map/all_to_all | solution.py:17
  58.9 4.1 %all-to-all-done.6 = bf16[8,32,512]{2,1,0:T(8,128)(2,1)S(1)} async-done(((bf16[8,32,512]{2,1,0:T(8,128)(2,1)}), bf16[8,32,512]{2,1,0:T(8,128)(2,1)S(1)}, u32[]{:S(2)}, u32[]{:S(2)}) %all-to-all-start.6) | async-done | bytes 262176 | tf_op jit(solution)/shard_map/all_to_all | solution.py:17
  63.0 4.4 %broadcast_in_dim.99 = bf16[8,768,512]{2,1,0:T(8,128)(2,1)} broadcast(bf16[768,512]{1,0:T(8,128)(2,1)} %broadcast_in_dim.98), dimensions={1,2} | broadcast | bytes 7077888 | tf_op jit(solution)/shard_map/broadcast_in_dim | solution.py:18
  67.4 5.7 %all-to-all-start.2 = ((bf16[8,768,512]{2,1,0:T(8,128)(2,1)}), bf16[8,768,512]{2,1,0:T(8,128)(2,1)}, u32[]{:S(2)}, u32[]{:S(2)}) async-start(bf16[8,768,512]{2,1,0:T(8,128)(2,1)} %broadcast_in_dim.99), calls=%async_computation.2 | async-start | bytes 12582912 | tf_op jit(solution)/shard_map/all_to_all | solution.py:17
  73.0 6.2 %copy.105 = bf16[2,128,4096]{1,0,2:T(2,128)(2,1)} copy(bf16[2,128,4096]{2,1,0:T(8,128)(2,1)} %param.18) | data formatting | bytes 4194304 | tf_op args[7]
  79.2 65.1 %all-to-all-done.2 = bf16[8,768,512]{2,1,0:T(8,128)(2,1)} async-done(((bf16[8,768,512]{2,1,0:T(8,128)(2,1)}), bf16[8,768,512]{2,1,0:T(8,128)(2,1)}, u32[]{:S(2)}, u32[]{:S(2)}) %all-to-all-start.2) | async-done | bytes 6291488 | tf_op jit(solution)/shard_map/all_to_all | solution.py:17
  144.3 5.2 %all-to-all-start.4 = ((bf16[2,128,4096]{1,0,2:T(2,128)(2,1)}), bf16[2,128,4096]{1,0,2:T(2,128)(2,1)}, u32[]{:S(2)}, u32[]{:S(2)}) async-start(bf16[2,128,4096]{1,0,2:T(2,128)(2,1)} %copy.105), calls=%async_computation.4 | async-start | bytes 4194304 | tf_op jit(solution)/shard_map/all_to_all | solution.py:127
  149.5 9.0 %copy.101 = bf16[768,8,512]{2,1,0:T(8,128)(2,1)} copy(bf16[768,8,512]{2,0,1:T(8,128)(2,1)} %bitcast.2) | data formatting | bytes 12582912 | tf_op jit(solution)/shard_map/transpose | solution.py:12
  158.6 12.0 %reshape_reshape.3 = bf16[32,2,12,4096]{3,2,1,0:T(8,128)(2,1)} reshape(bf16[768,8,512]{2,1,0:T(8,128)(2,1)} %copy.101) | data formatting | bytes 12582912 | tf_op jit(solution)/shard_map/reshape;reshape | solution.py:53
  170.6 7.9 %fusion.15 = f32[32,2,12,128]{3,0,2,1:T(8,128)S(1)} fusion(bf16[2,4096,128]{2,1,0:T(8,128)(2,1)S(1)} %copy-done, bf16[32,2,12,4096]{3,2,1,0:T(8,128)(2,1)} %reshape_reshape.3), kind=kOutput, calls=%fused_computation.14 | convolution fusion | flops 805306368 | bytes 8781824 | tf_op jit(solution)/shard_map/gecd,edf->gecf/dot_general | solution.py:43
  178.5 4.3 %fusion.30 = bf16[32,2,12,128]{3,0,2,1:T(8,128)(2,1)S(1)} fusion(bf16[2,4096,128]{2,1,0:T(8,128)(2,1)S(1)} %copy-done.5, bf16[32,2,12,4096]{3,2,1,0:T(8,128)(2,1)S(1)} %copy-done.1, f32[32,2,12,128]{3,0,2,1:T(8,128)S(1)} %fusion.15), kind=kOutput, calls=%fused_computation.17 | convolution fusion | flops 805896192 | bytes 8978432 | tf_op jit(solution)/shard_map/gecd,edf->gecf/dot_general | solution.py:46
  184.3 4.9 %all-to-all-start.3 = ((bf16[8,32,2,12,128]{4,1,3,2,0:T(8,128)(2,1)}), bf16[8,32,2,12,128]{4,1,3,2,0:T(8,128)(2,1)}, u32[]{:S(2)}, u32[]{:S(2)}) async-start(bf16[8,32,2,12,128]{4,1,3,2,0:T(8,128)(2,1)} %broadcast_in_dim.100), calls=%async_computation.3 | async-start | bytes 3145728 | tf_op jit(solution)/shard_map/all_to_all | solution.py:17
  190.5 2.1 convolution_convert_fusion
  193.4 6.1 %copy.106 = bf16[2,128,8,512]{3,1,2,0:T(8,128)(2,1)} copy(bf16[2,128,8,512]{1,0,3,2:T(2,128)(2,1)} %bitcast.10) | data formatting | bytes 4194304 | tf_op jit(solution)/shard_map/all_to_all | solution.py:127
  199.5 10.5 %all-to-all-done.3 = bf16[8,32,2,12,128]{4,1,3,2,0:T(8,128)(2,1)} async-done(((bf16[8,32,2,12,128]{4,1,3,2,0:T(8,128)(2,1)}), bf16[8,32,2,12,128]{4,1,3,2,0:T(8,128)(2,1)}, u32[]{:S(2)}, u32[]{:S(2)}) %all-to-all-start.3) | async-done | bytes 1572896 | tf_op jit(solution)/shard_map/all_to_all | solution.py:17
  210.0 4.3 %all-to-all-start.7 = ((bf16[8,32,512]{2,1,0:T(8,128)(2,1)}), bf16[8,32,512]{2,1,0:T(8,128)(2,1)S(1)}, u32[]{:S(2)}, u32[]{:S(2)}) async-start(bf16[8,32,512]{2,1,0:T(8,128)(2,1)} %bitcast.94), calls=%async_computation.7 | async-start | bytes 524288 | tf_op jit(solution)/shard_map/all_to_all | solution.py:38
  214.2 3.0 %fusion.12 = bf16[32,2,12,512]{3,0,2,1:T(8,128)(2,1)S(1)} fusion(bf16[2,1024,512,1]{2,1,3,0:T(8,128)(2,1)} %bitcast.97, bf16[8,32,2,12,128]{4,1,3,2,0:T(8,128)(2,1)} %all-to-all-done.3), kind=kOutput, calls=%fused_computation.13 | convolution fusion | flops 805699584 | bytes 4456448 | tf_op jit(solution)/shard_map/gecf,efd->gecd/dot_general | solution.py:134
  220.7 4.9 %all-to-all-start.5 = ((bf16[32,2,12,512]{3,1,2,0:T(2,128)(2,1)}), bf16[32,2,12,512]{3,1,2,0:T(2,128)(2,1)S(1)}, u32[]{:S(2)}, u32[]{:S(2)}) async-start(bf16[32,2,12,512]{3,1,2,0:T(2,128)(2,1)} %copy.107), calls=%async_computation.5 | async-start | bytes 1572864 | tf_op jit(solution)/shard_map/all_to_all | solution.py:137
  226.0 20.5 %all-to-all-done.5 = bf16[32,2,12,512]{3,1,2,0:T(2,128)(2,1)S(1)} async-done(((bf16[32,2,12,512]{3,1,2,0:T(2,128)(2,1)}), bf16[32,2,12,512]{3,1,2,0:T(2,128)(2,1)S(1)}, u32[]{:S(2)}, u32[]{:S(2)}) %all-to-all-start.5) | async-done | bytes 786464 | tf_op jit(solution)/shard_map/all_to_all | solution.py:137
  246.7 2.3 copy.109
  249.0 2.6 %reshape.167 = f32[768,512]{1,0:T(8,128)} reshape(f32[32,2,12,512]{3,2,1,0:T(8,128)} %copy.109) | data formatting | bytes 3145728 | tf_op jit(solution)/shard_map/reshape | solution.py:82
  251.6 2.6 %gather_fusion = f32[256,512]{1,0:T(8,128)S(1)} fusion(f32[768,512]{1,0:T(8,128)} %reshape.167, s32[1024]{0:T(1024)S(1)} %pad_clamp_fusion), kind=kCustom, calls=%fused_computation | custom fusion | bytes 1049600 | tf_op jit(solution)/shard_map/jit(_take)/gather | solution.py:84
  (65 shorter events, 22.0 us)
Async XLA Ops:
  0.0 170.6 %copy-start = (bf16[2,4096,128]{2,1,0:T(8,128)(2,1)S(1)}, bf16[2,4096,128]{2,1,0:T(8,128)(2,1)}, u32[]{:S(2)}) copy-start(bf16[2,4096,128]{2,1,0:T(8,128)(2,1)} %param.16) | copy-start | bytes 6291460
  1.6 11.0 %all-to-all-start = ((f32[8,1,32]{2,1,0:T(1,128)}), f32[8,1,32]{2,1,0:T(1,128)S(1)}, u32[]{:S(2)}, u32[]{:S(2)}) async-start(f32[8,1,32]{2,1,0:T(1,128)} %broadcast_in_dim.97), calls=%async_computation | async-start | bytes 8192 | tf_op jit(solution)/shard_map/all_to_all | solution.py:17
  49.1 13.9 %all-to-all-start.6 = ((bf16[8,32,512]{2,1,0:T(8,128)(2,1)}), bf16[8,32,512]{2,1,0:T(8,128)(2,1)S(1)}, u32[]{:S(2)}, u32[]{:S(2)}) async-start(bf16[8,32,512]{2,1,0:T(8,128)(2,1)} %broadcast_in_dim.103), calls=%async_computation.6 | async-start | bytes 524288 | tf_op jit(solution)/shard_map/all_to_all | solution.py:17
  63.0 4.4 %copy-start.3 = (bf16[8,32,512]{2,1,0:T(8,128)(2,1)}, bf16[8,32,512]{2,1,0:T(8,128)(2,1)S(1)}, u32[]{:S(2)}) copy-start(bf16[8,32,512]{2,1,0:T(8,128)(2,1)S(1)} %all-to-all-done.6) | copy-start | bytes 786436
  67.4 76.9 %all-to-all-start.2 = ((bf16[8,768,512]{2,1,0:T(8,128)(2,1)}), bf16[8,768,512]{2,1,0:T(8,128)(2,1)}, u32[]{:S(2)}, u32[]{:S(2)}) async-start(bf16[8,768,512]{2,1,0:T(8,128)(2,1)} %broadcast_in_dim.99), calls=%async_computation.2 | async-start | bytes 12582912 | tf_op jit(solution)/shard_map/all_to_all | solution.py:17
  144.3 38.5 %all-to-all-start.4 = ((bf16[2,128,4096]{1,0,2:T(2,128)(2,1)}), bf16[2,128,4096]{1,0,2:T(2,128)(2,1)}, u32[]{:S(2)}, u32[]{:S(2)}) async-start(bf16[2,128,4096]{1,0,2:T(2,128)(2,1)} %copy.105), calls=%async_computation.4 | async-start | bytes 4194304 | tf_op jit(solution)/shard_map/all_to_all | solution.py:127
  170.6 7.9 %copy-start.1 = (bf16[32,2,12,4096]{3,2,1,0:T(8,128)(2,1)S(1)}, bf16[32,2,12,4096]{3,2,1,0:T(8,128)(2,1)}, u32[]{:S(2)}) copy-start(bf16[32,2,12,4096]{3,2,1,0:T(8,128)(2,1)} %reshape_reshape.3) | copy-start | bytes 18874372
  170.6 7.9 %copy-start.5 = (bf16[2,4096,128]{2,1,0:T(8,128)(2,1)S(1)}, bf16[2,4096,128]{2,1,0:T(8,128)(2,1)}, u32[]{:S(2)}) copy-start(bf16[2,4096,128]{2,1,0:T(8,128)(2,1)} %param.17) | copy-start | bytes 6291460
  184.3 5.9 %copy-start.2 = (bf16[4096,128]{1,0:T(8,128)(2,1)S(1)}, bf16[4096,128]{1,0:T(8,128)(2,1)}, u32[]{:S(2)}) copy-start(bf16[4096,128]{1,0:T(8,128)(2,1)} %param.19) | copy-start | bytes 3145732
  184.3 25.6 %all-to-all-start.3 = ((bf16[8,32,2,12,128]{4,1,3,2,0:T(8,128)(2,1)}), bf16[8,32,2,12,128]{4,1,3,2,0:T(8,128)(2,1)}, u32[]{:S(2)}, u32[]{:S(2)}) async-start(bf16[8,32,2,12,128]{4,1,3,2,0:T(8,128)(2,1)} %broadcast_in_dim.100), calls=%async_computation.3 | async-start | bytes 3145728 | tf_op jit(solution)/shard_map/all_to_all | solution.py:17
  210.0 10.8 %all-to-all-start.7 = ((bf16[8,32,512]{2,1,0:T(8,128)(2,1)}), bf16[8,32,512]{2,1,0:T(8,128)(2,1)S(1)}, u32[]{:S(2)}, u32[]{:S(2)}) async-start(bf16[8,32,512]{2,1,0:T(8,128)(2,1)} %bitcast.94), calls=%async_computation.7 | async-start | bytes 524288 | tf_op jit(solution)/shard_map/all_to_all | solution.py:38
  217.3 8.5 %copy-start.4 = (f32[32,8]{0,1:T(8,128)S(1)}, f32[32,8]{0,1:T(8,128)}, u32[]{:S(2)}) copy-start(f32[32,8]{0,1:T(8,128)} %param.14) | copy-start | bytes 3076
  220.7 25.7 %all-to-all-start.5 = ((bf16[32,2,12,512]{3,1,2,0:T(2,128)(2,1)}), bf16[32,2,12,512]{3,1,2,0:T(2,128)(2,1)S(1)}, u32[]{:S(2)}, u32[]{:S(2)}) async-start(bf16[32,2,12,512]{3,1,2,0:T(2,128)(2,1)} %copy.107), calls=%async_computation.5 | async-start | bytes 1572864 | tf_op jit(solution)/shard_map/all_to_all | solution.py:137
where the time goes:
time: 258 us; the launch traced here: 255 us
  waiting for transfers between devices  102 us (40%)
  local copies, waits for them, and re-layouts  59.4 us (23%)
  starting transfers between devices  38.7 us (15%)
  blocking collectives  31.5 us (12%)
  matrix products  18.9 us (7%)
  other arithmetic  4.39 us (2%)
    all_to_all x4, waiting for transfers between devices, sent_to_all(): lax.all_to_all(jnp.broadcast_to(value[None], (size, *value.shape)), axis,...  79.7 us
    all_to_all x1, blocking collectives, body(): lax.all_to_all(outgoing, 'ep', split_axis=0, concat_axis=0, tiled=True)  31.5 us
    all_to_all x4, starting transfers between devices, sent_to_all(): lax.all_to_all(jnp.broadcast_to(value[None], (size, *value.shape)), axis,...  24.4 us
    all_to_all x1, waiting for transfers between devices, body(): lax.all_to_all(result.astype(jnp.bfloat16), 'ep', split_axis=0, concat_ax...  20.5 us
    another operation x1, local copies, waits for them, and re-layouts, widen_rows(): return widened.reshape(arrived.shape[:-1] + (widened.shape[1],))  12 us
    transpose x1, local copies, waits for them, and re-layouts, in_order(): return jnp.moveaxis(tiles, 0, dim).reshape(lengths)  9.03 us
    broadcast_in_dim x5, local copies, waits for them, and re-layouts, sent_to_all(): jnp.broadcast_to(value[None], (size, *value.shape))  8.3 us
    dot_general x1, matrix products, expert_inner(): jnp.einsum('gecd,edf->gecf', arrived, gate_proj, preferred_element_type=j...  7.86 us
  transfers between devices with their start and end apart: 7, of which 5 were waited for; matrix products, arithmetic and copies ran while one was open for 24% of the time, Pallas kernels for 0%

commit v1 on v0

v1 whole, which is shorter than its diff:
```python
import functools

import jax
import jax.numpy as jnp
from jax import lax
from jax.experimental import pallas as pl
from jax.experimental.pallas import tpu as pltpu
from jax.sharding import PartitionSpec as P

MESH = pl.DeviceIdType.MESH
EPS = 1e-06
NZ, NX, NY = 8, 4, 4
BLK = 16
HALF = 512
F32, BF16 = jnp.float32, jnp.bfloat16
SEQ = (0, 1, 7, 2, 6, 3, 5, 4)
POS = {dz: i for i, dz in enumerate(SEQ)}


class Ids:
    def __init__(self):
        self.table, self.count = {}, 0

    def at(self, *key):
        if key not in self.table:
            self.table[key] = self.count
            self.count += 1
        return self.table[key]


def build_ids():
    ids = Ids()
    for p in range(NZ):
        for h in range(2):
            ids.at("z", p, h)
    for p in range(NZ):
        ids.at("zr", p)
        for r in (1, 2, 3):
            ids.at("br", p, r)
            for h in range(2):
                for stage in ("ab", "ac", "rc", "rb"):
                    ids.at(stage, p, h, r)
        for c in range(2):
            ids.at("rz", p, c)
    for k in range(8):
        ids.at("gain", k)
    for k in range(9):
        ids.at("w", k)
    return ids


IDS = build_ids()


def kernel(
    hidden_ref, gain_ref, eid_ref, rw_ref, len_ref, gate_ref, up_ref, down_ref, sgate_ref, sup_ref, sdown_ref,
    out_ref,
    hbuf, pbuf, rbuf, rown, gbuf, hn, inner, wgu, wd, wsgu, wsd, fc0, fc1, fb, zb, lsem, ssem, rsem,
):
    ep, tp = lax.axis_index("ep"), lax.axis_index("tp")
    z, x = ep // NX, ep % NX
    y, core = tp // 2, tp % 2
    other = 1 - core

    def dev(dz=0, dx=0, dy=0, c=None):
        c = core if c is None else c
        return (((z + dz) % NZ) * NX + (x + dx) % NX, ((y + dy) % NY) * 2 + c)

    started = []

    def push(src, dst, key, to, add=0):
        i = IDS.at(*key) + add
        cp = pltpu.make_async_remote_copy(
            src_ref=src, dst_ref=dst, send_sem=ssem.at[i], recv_sem=rsem.at[i], device_id=to, device_id_type=MESH
        )
        cp.start()
        started.append(cp)

    def arrive(dst, key, add=0):
        i = IDS.at(*key) + add
        pltpu.make_async_remote_copy(
            src_ref=dst, dst_ref=dst, send_sem=ssem.at[i], recv_sem=rsem.at[i], device_id=dev(c=other), device_id_type=MESH
        ).wait_recv()

    def lanes(first):
        return pl.ds(pl.multiple_of(first + core * 128, 128), 128)

    weights = []
    for e in range(2):
        weights.append((gate_ref.at[e], wgu.at[:, lanes(e * 256)]))
        weights.append((up_ref.at[e], wgu.at[:, lanes(512 + e * 256)]))
    weights.append((sgate_ref, wsgu.at[:, lanes(0)]))
    weights.append((sup_ref, wsgu.at[:, lanes(256)]))
    for e in range(2):
        weights.append((down_ref.at[e], wd.at[lanes(e * 256), :]))
    weights.append((sdown_ref, wsd.at[lanes(0), :]))
    local = [pltpu.make_async_copy(s, d, lsem.at[k]) for k, (s, d) in enumerate(weights)]
    for cp in local:
        cp.start()

    barrier = pltpu.get_barrier_semaphore()
    peers = [dev(dz=o, c=c) for o in range(1, NZ) for c in range(2)] + [dev(c=other)]
    peers += [dev(dy=o, c=c) for o in range(1, NY) for c in range(2)]
    peers += [dev(dx=1), dev(dx=-1 + NX)]
    for peer in peers:
        pl.semaphore_signal(barrier, inc=1, device_id=peer, device_id_type=MESH)

    lane = lax.broadcasted_iota(jnp.int32, (32, 128), 1)
    row = lax.broadcasted_iota(jnp.int32, (32, 128), 0)
    seq_len = jnp.zeros((32, 128), jnp.int32)
    for q in range(4):
        seq_len = jnp.where(row // 8 == q, len_ref[q], seq_len)
    live = row % 8 < seq_len
    mix = jnp.zeros((32, 128), F32)
    for k in range(8):
        mix = mix + jnp.where(eid_ref[:, k : k + 1] == lane % 64, rw_ref[:, k : k + 1], 0.0)
    mix = jnp.where(live, mix, 0.0)
    high = mix.astype(BF16).astype(F32)
    terms = jnp.where(lane < 64, high, mix - high).astype(BF16)
    rown[...] = terms.reshape(2, BLK, 128)
    rbuf[0, 0:BLK, :] = rown[core]
    gbuf[tp] = gain_ref[...]
    hbuf[core, 0, 0:BLK, 0:HALF] = hidden_ref[core]

    pl.semaphore_wait(barrier, len(peers))

    for o in (1, 7, 2, 6, 3, 5, 4):
        p = POS[(-o) % NZ]
        if o == 1:
            push(hidden_ref.at[other], hbuf.at[core, 0, 0:BLK, 0:HALF], ("z", 0, 0), dev(c=other), core)
        for c in range(2):
            push(hidden_ref.at[c], hbuf.at[core, p, 0:BLK, 0:HALF], ("z", p, 0), dev(dz=o, c=c), core)
        push(rown.at[core], rbuf.at[p, 0:BLK, :], ("zr", p), dev(dz=o))
    for k, (s, d) in enumerate(weights):
        if k < 4:
            push(s, d, ("w", k), dev(c=other))
    for o in range(NY):
        for c in range(2):
            if o > 0:
                push(gbuf.at[tp], gbuf.at[tp], ("gain", 0), dev(dy=o, c=c), tp)
    push(gbuf.at[tp], gbuf.at[tp], ("gain", 0), dev(c=other), tp)
    for k, (s, d) in enumerate(weights):
        if k >= 4:
            push(s, d, ("w", k), dev(c=other))

    def bslice(ref, p, h, r):
        if h == 0:
            return ref.at[h, p, 0:BLK, r * HALF : (r + 1) * HALF]
        return ref.at[h, p, r * BLK : (r + 1) * BLK, 0:HALF]

    def cslice(ref, p, h, r):
        if h == 0:
            return ref.at[h, p, r * BLK : (r + 1) * BLK, :]
        return ref.at[h, p, :, r * HALF : (r + 1) * HALF]

    def along(stage, h, step):
        on_y = (stage == "b") == (h == 0)
        return dev(dy=step % NY) if on_y else dev(dx=step % NX)

    def ring_first(view, stage, key, p, h, ref):
        push(view(ref, p, h, 0), view(ref, p, h, 3), (key, p, h, 3), along(stage, h, 1))
        push(view(ref, p, h, 0), view(ref, p, h, 1), (key, p, h, 1), along(stage, h, -1))

    def ring_forward(view, stage, key, p, h, ref):
        near, step = (3, 1) if p % 2 == 0 else (1, -1)
        arrive(view(ref, p, h, near), (key, p, h, near))
        push(view(ref, p, h, near), view(ref, p, h, 2), (key, p, h, 2), along(stage, h, step))
        arrive(view(ref, p, h, 4 - near), (key, p, h, 4 - near))

    def rslice(p, r):
        return rbuf.at[p, r * BLK : (r + 1) * BLK, :]

    def stage_a(p):
        for h in range(2):
            if p > 0:
                arrive(hbuf.at[h, p, 0:BLK, 0:HALF], ("z", p, h))
        if p == 0:
            arrive(hbuf.at[other, 0, 0:BLK, 0:HALF], ("z", 0, 0), other)
        else:
            arrive(rslice(p, 0), ("zr", p))
        for h in range(2):
            ring_first(bslice, "b", "ab", p, h, hbuf)
        push(rslice(p, 0), rslice(p, 3), ("br", p, 3), dev(dx=1))
        push(rslice(p, 0), rslice(p, 1), ("br", p, 1), dev(dx=3))

    def stage_b(p):
        for h in range(2):
            ring_forward(bslice, "b", "ab", p, h, hbuf)
        near, step = (3, 1) if p % 2 == 0 else (1, 3)
        arrive(rslice(p, near), ("br", p, near))
        push(rslice(p, near), rslice(p, 2), ("br", p, 2), dev(dx=step))
        arrive(rslice(p, 4 - near), ("br", p, 4 - near))

    def stage_c(p):
        for h in range(2):
            arrive(bslice(hbuf, p, h, 2), ("ab", p, h, 2))
            ring_first(cslice, "c", "ac", p, h, hbuf)
        arrive(rslice(p, 2), ("br", p, 2))

    def stage_d(p):
        for h in range(2):
            ring_forward(cslice, "c", "ac", p, h, hbuf)

    def stage_e(p):
        for h in range(2):
            arrive(cslice(hbuf, p, h, 2), ("ac", p, h, 2))

    def weight_ready(ks):
        for k in ks:
            local[k].wait()
            arrive(partner[k], ("w", k))

    def plan_partner():
        def lo(first):
            return pl.ds(pl.multiple_of(first + other * 128, 128), 128)

        out = []
        for e in range(2):
            out += [wgu.at[:, lo(e * 256)], wgu.at[:, lo(512 + e * 256)]]
        out += [wsgu.at[:, lo(0)], wsgu.at[:, lo(256)]]
        out += [wd.at[lo(e * 256), :] for e in range(2)]
        return out + [wsd.at[lo(0), :]]

    partner = plan_partner()

    def dot(a, b):
        return jnp.dot(a, b, preferred_element_type=F32)

    def columns(h, r):
        return pl.ds(pl.multiple_of(((y + r) % NY) * 1024 + h * HALF, HALF), HALF)

    def silu(v):
        return v / (1.0 + jnp.exp(-v))

    def compute(g, planes):
        first = g * planes
        rows = planes * 64
        if g == 0:
            for o in range(NY):
                for c in range(2):
                    if o > 0:
                        k = ((y + o) % NY) * 2 + c
                        arrive(gbuf.at[k], ("gain", 0), k)
            k = y * 2 + other
            arrive(gbuf.at[k], ("gain", 0), k)

        def normalise(b, carry):
            p = first + b // 4
            at = pl.ds(pl.multiple_of((b % 4) * BLK, BLK), BLK)
            to = pl.ds(pl.multiple_of(b * BLK, BLK), BLK)
            squares = jnp.zeros((BLK, HALF), F32)
            for h in range(2):
                for r in range(NY):
                    v = hbuf[h, p, at, r * HALF : (r + 1) * HALF].astype(F32)
                    squares = squares + v * v
            scale = lax.rsqrt(jnp.sum(squares, axis=1, keepdims=True) / 4096.0 + EPS)
            for h in range(2):
                for r in range(NY):
                    v = hbuf[h, p, at, r * HALF : (r + 1) * HALF].astype(F32)
                    gain = gbuf[((y + r) % NY) * 2 + h]
                    hn[to, columns(h, r)] = (v * scale * gain).astype(BF16)
            return carry

        lax.fori_loop(0, rows // BLK, normalise, 0)
        if g == 0:
            weight_ready(range(0, 4))
        route = rbuf[first : first + planes].reshape(rows, 128)
        pick_row = lax.broadcasted_iota(jnp.int32, (128, 256), 0) % 64
        for e in range(2):
            pick = jnp.where(pick_row == ep * 2 + e, 1.0, 0.0).astype(BF16)
            share = dot(route, pick)
            gate = dot(hn[...], wgu[:, e * 256 : (e + 1) * 256])
            up = dot(hn[...], wgu[:, 512 + e * 256 : 768 + e * 256])
            inner[:, e * 256 : (e + 1) * 256] = (silu(gate) * up * share).astype(BF16)
        if g == 0:
            weight_ready(range(4, 9))
            own = hn[0:BLK, :]
            shared = (silu(dot(own, wsgu[:, 0:256])) * dot(own, wsgu[:, 256:512])).astype(BF16)
        for h in range(2):
            for r in range(NY):
                part = dot(inner[...], wd[:, columns(h, r)])
                cols = slice(r * HALF, (r + 1) * HALF)
                pbuf[h, first : first + planes, :, cols] = part.reshape(planes, 64, HALF).astype(BF16)
                if g == 0:
                    extra = dot(shared, wsd[:, columns(h, r)])
                    pbuf[h, 0, 0:BLK, cols] = (part[0:BLK] + extra).astype(BF16)

    def land(stage, p, h, r):
        if stage == "b":
            return fb.at[h, p, r - 1]
        return (fc0 if h == 0 else fc1).at[p, r - 1]

    def sum_first(view, stage, key, p, h):
        near, step = (1, 1) if p % 2 == 0 else (3, -1)
        push(view(pbuf, p, h, 2), land(stage, p, h, 2), (key, p, h, 2), along(stage, h, step))
        push(view(pbuf, p, h, 4 - near), land(stage, p, h, near), (key, p, h, near), along(stage, h, -step))

    def sum_forward(view, stage, key, p, h):
        near, step = (1, 1) if p % 2 == 0 else (3, -1)
        arrive(land(stage, p, h, 2), (key, p, h, 2))
        mine = view(pbuf, p, h, near)
        mine[...] = (mine[...].astype(F32) + land(stage, p, h, 2)[...].astype(F32)).astype(BF16)
        push(mine, land(stage, p, h, 4 - near), (key, p, h, 4 - near), along(stage, h, step))

    def sum_last(view, stage, key, p, h):
        for r in (1, 3):
            arrive(land(stage, p, h, r), (key, p, h, r))
        mine = view(pbuf, p, h, 0)
        mine[...] = (
            mine[...].astype(F32) + land(stage, p, h, 1)[...].astype(F32) + land(stage, p, h, 3)[...].astype(F32)
        ).astype(BF16)

    def stage_r1(p):
        for h in range(2):
            sum_first(cslice, "c", "rc", p, h)

    def stage_r2(p):
        for h in range(2):
            sum_forward(cslice, "c", "rc", p, h)

    def stage_r3(p):
        for h in range(2):
            sum_last(cslice, "c", "rc", p, h)
            sum_first(bslice, "b", "rb", p, h)

    def stage_r4(p):
        for h in range(2):
            sum_forward(bslice, "b", "rb", p, h)

    def stage_r5(p):
        for h in range(2):
            sum_last(bslice, "b", "rb", p, h)
        dz = SEQ[p]
        q = POS[(-dz) % NZ]
        if p == 0:
            zb[0, core] = pbuf[core, 0, 0:BLK, 0:HALF]
            push(pbuf.at[other, 0, 0:BLK, 0:HALF], zb.at[0, core], ("rz", 0, 0), dev(c=other), core)
        else:
            for h in range(2):
                push(pbuf.at[h, p, 0:BLK, 0:HALF], zb.at[q, core], ("rz", q, 0), dev(dz=dz, c=h), core)

    planes = 2
    stages = (stage_a, stage_b, stage_c, stage_d, stage_e)
    back = (stage_r2, stage_r3, stage_r4, stage_r5)
    ready = {}
    for tick in range(NZ + 4 + len(back)):
        for k in range(len(back) - 1, -1, -1):
            for p in range(NZ):
                if ready.get(p) == tick - 1 - k:
                    back[k](p)
        for k in range(4, -1, -1):
            if 0 <= tick - k < NZ:
                stages[k](tick - k)
        last = tick - 4
        if 0 <= last < NZ and (last + 1) % planes == 0:
            g = last // planes
            compute(g, planes)
            for p in range(g * planes, (g + 1) * planes):
                stage_r1(p)
                ready[p] = tick

    for p in range(1, NZ):
        for c in range(2):
            arrive(zb.at[p, c], ("rz", p, c))
    arrive(zb.at[0, other], ("rz", 0, 0), other)
    for c in range(2):
        total = zb[0, c].astype(F32)
        for p in range(1, NZ):
            total = total + zb[p, c].astype(F32)
        alive = live[c * BLK : (c + 1) * BLK, 0:1]
        out_ref[c] = jnp.where(alive, total, 0.0).astype(BF16)
    for cp in started:
        cp.wait_send()


def body(hidden, norm_gain, expert_ids, route_weights, lengths, gate_proj, up_proj, down_proj, sgate, sup, sdown):
    vmem = pl.BlockSpec(memory_space=pltpu.VMEM)
    anywhere = pl.BlockSpec(memory_space=pl.ANY)
    n = IDS.count
    out = pl.pallas_call(
        kernel,
        out_shape=jax.ShapeDtypeStruct((2, BLK, HALF), BF16),
        in_specs=[vmem] * 4 + [pl.BlockSpec(memory_space=pltpu.SMEM)] + [anywhere] * 6,
        out_specs=vmem,
        scratch_shapes=[
            pltpu.VMEM((2, NZ, 64, 2048), BF16),
            pltpu.VMEM((2, NZ, 64, 2048), BF16),
            pltpu.VMEM((NZ, 64, 128), BF16),
            pltpu.VMEM((2, BLK, 128), BF16),
            pltpu.VMEM((8, 1, HALF), F32),
            pltpu.VMEM((128, 4096), BF16),
            pltpu.VMEM((128, 512), BF16),
            pltpu.VMEM((4096, 1024), BF16),
            pltpu.VMEM((512, 4096), BF16),
            pltpu.VMEM((4096, 512), BF16),
            pltpu.VMEM((256, 4096), BF16),
            pltpu.VMEM((NZ, 3, BLK, 2048), BF16),
            pltpu.VMEM((NZ, 3, 64, HALF), BF16),
            pltpu.VMEM((2, NZ, 3, BLK, HALF), BF16),
            pltpu.VMEM((NZ, 2, BLK, HALF), BF16),
            pltpu.SemaphoreType.DMA((9,)),
            pltpu.SemaphoreType.DMA((n,)),
            pltpu.SemaphoreType.DMA((n,)),
        ],
        compiler_params=pltpu.CompilerParams(
            collective_id=0, has_side_effects=True, vmem_limit_bytes=60 * 1024 * 1024
        ),
    )(
        hidden.reshape(2, BLK, HALF),
        norm_gain.reshape(1, HALF),
        expert_ids,
        route_weights,
        lengths,
        gate_proj,
        up_proj,
        down_proj,
        sgate,
        sup,
        sdown,
    )
    return out.reshape(2 * BLK, HALF)


def solution(mesh):
    placed = (
        P("ep", "tp"),
        P("tp"),
        P("ep", None),
        P("ep", None),
        P("ep"),
        P("ep", None, "tp"),
        P("ep", None, "tp"),
        P("ep", "tp", None),
        P(None, "tp"),
        P(None, "tp"),
        P("tp", None),
    )
    return jax.shard_map(body, mesh=mesh, in_specs=placed, out_specs=P("ep", "tp"), check_vma=False)
```

time: 258 us -> 106 us (0.41)
  waiting for transfers between devices: 102 us -> 0 us
  Pallas kernels: 0 us -> 101 us
  local copies, waits for them, and re-layouts: 59.4 us -> 4.1 us
  starting transfers between devices: 38.7 us -> 0 us
  blocking collectives: 31.5 us -> 0 us
  matrix products: 18.9 us -> 0 us
  other arithmetic: 4.39 us -> 0 us
    all_to_all x7 -> x0, waiting for transfers between devices: 102 us -> none  [the longest x4 79.7 us: sent_to_all(): lax.all_to_all(jnp.broadcast_to(value[None], (size, *value.shape)), axis,...]
    pallas_call x0 -> x1, Pallas kernels: none -> 101 us  [body(): pl.pallas_call(kernel, out_shape=jax.ShapeDtypeStruct((2, BLK, HALF), BF1...]
    all_to_all x7 -> x0, starting transfers between devices: 38.7 us -> none  [the longest x4 24.4 us: sent_to_all(): lax.all_to_all(jnp.broadcast_to(value[None], (size, *value.shape)), axis,...]
    all_to_all x1 -> x0, blocking collectives: 31.5 us -> none  [body(): lax.all_to_all(outgoing, 'ep', split_axis=0, concat_axis=0, tiled=True)]
    dot_general x6 -> x0, matrix products: 18.9 us -> none  [the longest x1 7.86 us: expert_inner(): jnp.einsum('gecd,edf->gecf', arrived, gate_proj, preferred_element_type=j...]
    another operation x2 -> x0, local copies, waits for them, and re-layouts: 12 us -> none  [the longest x1 12 us: widen_rows(): return widened.reshape(arrived.shape[:-1] + (widened.shape[1],))]
    broadcast_in_dim x12 -> x0, local copies, waits for them, and re-layouts: 10.2 us -> none  [the longest x5 8.3 us: sent_to_all(): jnp.broadcast_to(value[None], (size, *value.shape))]
    transpose x1 -> x0, local copies, waits for them, and re-layouts: 9.03 us -> none  [in_order(): return jnp.moveaxis(tiles, 0, dim).reshape(lengths)]
  transfers between devices with their start and end apart: 7 -> 0, of which waited for: 5 -> 0; matrix products, arithmetic and copies ran while one was open for 24% -> 0% of each run, Pallas kernels for 0% -> 0%
where the time goes in v1:
time: 106 us; the launch traced here: 105 us
  Pallas kernels  101 us (95%)
  local copies, waits for them, and re-layouts  4.1 us (4%)
    pallas_call x1, Pallas kernels, body(): pl.pallas_call(kernel, out_shape=jax.ShapeDtypeStruct((2, BLK, HALF), BF1...  101 us
    unnamed x3, local copies, waits for them, and re-layouts  4.1 us

profile of v1, /device:TPU:1, one launch (start us, length us, event | category | flops | bytes accessed | tf_op | source)
XLA Modules:
  0.0 105.4 jit_solution(10093929152023478950)
XLA Ops:
  0.0 1.4 %copy.12.eid_ref = s32[32,8]{1,0:T(8,128)} copy(s32[32,8]{0,1:T(8,128)} %param.13) | data formatting | bytes 2048 | tf_op args[2]
  1.4 1.4 %copy.13.rw_ref = f32[32,8]{1,0:T(8,128)} copy(f32[32,8]{0,1:T(8,128)} %param.14) | data formatting | bytes 2048 | tf_op args[3]
  2.7 101.3 %shard_map.109 = bf16[2,16,512]{2,1,0:T(8,128)(2,1)} custom-call(bf16[2,16,512]{2,1,0:T(8,128)(2,1)} %bitcast.4, f32[1,512]{1,0:T(1,128)} %bitcast.5, s32[32,8]{1,0:T(8,128)} %copy.12.eid_ref, f32[32,8]{1,0:T(8,128)} %copy.13.rw_ref, s32[4]{0:T(128)} %len_ref.1, bf16[2,4096,128]{2,1,0:T(8,128)(2,1)} %gate_ref.1, bf16[2,4096,128]{2,1,0:T(8,128)(2,1)} %up_ref.1, ...), custom_call_target="tpu_custom_call" | custom-call | tf_op jit(solution)/shard_map/pallas_call | solution.py:380
  104.1 1.4 %copy.15 = bf16[32,512]{1,0:T(8,128)(2,1)} copy(bf16[32,512]{1,0:T(8,128)(2,1)} %bitcast.3) | data formatting | bytes 65536

commit v2 on v1

--- a/solution.py
+++ b/solution.py
@@ -17,6 +17,25 @@
 POS = {dz: i for i, dz in enumerate(SEQ)}
 
 
+GROUPS_OF = ((0, 1), (2, 3), (4, 5), (6, 7))
+ORDER = (
+    "a00", "a01", "i0", "a11", "a10", "i1", "b00", "b01", "j0", "a20", "a21", "i2", "a30", "a31", "i3", "b11",
+    "b10", "j1", "a50", "i5", "a40", "a51", "a41", "i4", "c00", "c01", "k0", "b20", "b21", "j2", "a61", "i6",
+    "a60", "b30", "a71", "a70", "i7", "j3", "b31", "c10", "c11", "k1", "j5", "b50", "b40", "b41", "b51", "j4",
+    "d01", "d00", "c20", "c21", "k2", "b60", "c30", "b61", "j6", "b70", "b71", "j7", "k3", "c31", "d11", "c40",
+    "c50", "c41", "d10", "k4", "k5", "c51", "e01", "e00", "c70", "d21", "c60", "d20", "d31", "d30", "c71", "k7",
+    "e11", "c61", "k6", "d41", "d40", "d50", "d51", "e10", "n0", "m0", "d70", "v01", "d71", "d60", "v00", "r10",
+    "d61", "r00", "r01", "r11", "e31", "e21", "e20", "e30", "n1", "m1", "v10", "e51", "r30", "e40", "e60", "r20",
+    "e50", "v11", "r31", "r21", "e70", "e71", "e61", "n3", "m3", "v31", "r61", "v30", "r71", "r70", "r60", "e41",
+    "n2", "m2", "v21", "r41", "v20", "r40", "r51", "s31", "s11", "s21", "s20", "r50", "s10", "s30", "s61", "s01",
+    "s00", "s70", "s71", "s60", "s41", "s40", "s51", "t20", "s50", "t31", "t21", "t10", "t61", "t11", "t30", "t00",
+    "t71", "t01", "t70", "t60", "t51", "t41", "u20", "t50", "t40", "u10", "u31", "u30", "u21", "u00", "u61", "u11",
+    "u70", "u71", "u60", "u01", "u51", "w20", "u41", "u50", "w31", "u40", "w21", "w10", "w00", "w61", "w30", "w11",
+    "w70", "w71", "w60", "w01", "w51", "w41", "w50", "w40",
+)
+LAST_HALF = 1 if ORDER.index("w00") < ORDER.index("w01") else 0
+
+
 class Ids:
     def __init__(self):
         self.table, self.count = {}, 0
@@ -30,6 +49,8 @@
 
 def build_ids():
     ids = Ids()
+    for key in ("zp", "rzp"):
+        ids.count = ids.at(key) + 2
     for p in range(NZ):
         for h in range(2):
             ids.at("z", p, h)
@@ -50,12 +71,14 @@
 
 
 IDS = build_ids()
+RINGS = ("ab", "ac", "rb", "rc")
+GROUPS = [k + str(h) for k in RINGS for h in range(2)] + ["z", "zp", "zr", "br", "gain", "rz", "rzp", "w"]
 
 
 def kernel(
     hidden_ref, gain_ref, eid_ref, rw_ref, len_ref, gate_ref, up_ref, down_ref, sgate_ref, sup_ref, sdown_ref,
     out_ref,
-    hbuf, pbuf, rbuf, rown, gbuf, hn, inner, wgu, wd, wsgu, wsd, fc0, fc1, fb, zb, lsem, ssem, rsem,
+    hbuf, pbuf, rbuf, rown, gbuf, hn, inner, shared, wgu, wd, wsgu, wsd, fc0, fc1, fb, zb, lsem, wsem, ssem, rsem,
 ):
     ep, tp = lax.axis_index("ep"), lax.axis_index("tp")
     z, x = ep // NX, ep % NX
@@ -66,20 +89,27 @@
         c = core if c is None else c
         return (((z + dz) % NZ) * NX + (x + dx) % NX, ((y + dy) % NY) * 2 + c)
 
-    started = []
+    def group(key):
+        return GROUPS.index(key[0] + str(key[2]) if key[0] in RINGS else key[0])
 
     def push(src, dst, key, to, add=0):
         i = IDS.at(*key) + add
-        cp = pltpu.make_async_remote_copy(
-            src_ref=src, dst_ref=dst, send_sem=ssem.at[i], recv_sem=rsem.at[i], device_id=to, device_id_type=MESH
-        )
-        cp.start()
-        started.append(cp)
+        sem = ssem.at[group(key)]
+        if key[0] == "w":
+            sem = wsem.at[key[1]]
+        pltpu.make_async_remote_copy(
+            src_ref=src, dst_ref=dst, send_sem=sem, recv_sem=rsem.at[i], device_id=to, device_id_type=MESH
+        ).start()
+
+    def sent(ref, sem):
+        pltpu.make_async_remote_copy(
+            src_ref=ref, dst_ref=ref, send_sem=sem, recv_sem=rsem.at[0], device_id=dev(c=other), device_id_type=MESH
+        ).wait_send()
 
     def arrive(dst, key, add=0):
         i = IDS.at(*key) + add
         pltpu.make_async_remote_copy(
-            src_ref=dst, dst_ref=dst, send_sem=ssem.at[i], recv_sem=rsem.at[i], device_id=dev(c=other), device_id_type=MESH
+            src_ref=dst, dst_ref=dst, send_sem=ssem.at[0], recv_sem=rsem.at[i], device_id=dev(c=other), device_id_type=MESH
         ).wait_recv()
 
     def lanes(first):
@@ -105,29 +135,32 @@
     for peer in peers:
         pl.semaphore_signal(barrier, inc=1, device_id=peer, device_id_type=MESH)
 
-    lane = lax.broadcasted_iota(jnp.int32, (32, 128), 1)
-    row = lax.broadcasted_iota(jnp.int32, (32, 128), 0)
-    seq_len = jnp.zeros((32, 128), jnp.int32)
-    for q in range(4):
-        seq_len = jnp.where(row // 8 == q, len_ref[q], seq_len)
-    live = row % 8 < seq_len
-    mix = jnp.zeros((32, 128), F32)
+    def live_slots(shape, dim):
+        slot = lax.broadcasted_iota(jnp.int32, shape, dim)
+        seq_len = jnp.zeros(shape, jnp.int32)
+        for q in range(4):
+            seq_len = jnp.where(slot // 8 == q, len_ref[q], seq_len)
+        return slot % 8 < seq_len
+
+    expert = lax.broadcasted_iota(jnp.int32, (128, 32), 0)
+    mix = jnp.zeros((128, 32), F32)
     for k in range(8):
-        mix = mix + jnp.where(eid_ref[:, k : k + 1] == lane % 64, rw_ref[:, k : k + 1], 0.0)
-    mix = jnp.where(live, mix, 0.0)
+        mix = mix + jnp.where(eid_ref[k : k + 1, :] == expert % 64, rw_ref[k : k + 1, :], 0.0)
+    mix = jnp.where(live_slots((128, 32), 1), mix, 0.0)
     high = mix.astype(BF16).astype(F32)
-    terms = jnp.where(lane < 64, high, mix - high).astype(BF16)
-    rown[...] = terms.reshape(2, BLK, 128)
+    terms = jnp.where(expert < 64, high, mix - high).T
+    rown[...] = terms.reshape(2, BLK, 128).astype(BF16)
     rbuf[0, 0:BLK, :] = rown[core]
     gbuf[tp] = gain_ref[...]
     hbuf[core, 0, 0:BLK, 0:HALF] = hidden_ref[core]
 
-    pl.semaphore_wait(barrier, len(peers))
+    with jax.named_scope("barrier"):
+        pl.semaphore_wait(barrier, len(peers))
 
     for o in (1, 7, 2, 6, 3, 5, 4):
         p = POS[(-o) % NZ]
         if o == 1:
-            push(hidden_ref.at[other], hbuf.at[core, 0, 0:BLK, 0:HALF], ("z", 0, 0), dev(c=other), core)
+            push(hidden_ref.at[other], hbuf.at[core, 0, 0:BLK, 0:HALF], ("zp",), dev(c=other), core)
         for c in range(2):
             push(hidden_ref.at[c], hbuf.at[core, p, 0:BLK, 0:HALF], ("z", p, 0), dev(dz=o, c=c), core)
         push(rown.at[core], rbuf.at[p, 0:BLK, :], ("zr", p), dev(dz=o))
@@ -165,45 +198,50 @@
         near, step = (3, 1) if p % 2 == 0 else (1, -1)
         arrive(view(ref, p, h, near), (key, p, h, near))
         push(view(ref, p, h, near), view(ref, p, h, 2), (key, p, h, 2), along(stage, h, step))
+
+    def ring_done(view, key, p, h, ref):
+        near = 3 if p % 2 == 0 else 1
         arrive(view(ref, p, h, 4 - near), (key, p, h, 4 - near))
+        arrive(view(ref, p, h, 2), (key, p, h, 2))
 
     def rslice(p, r):
         return rbuf.at[p, r * BLK : (r + 1) * BLK, :]
 
-    def stage_a(p):
-        for h in range(2):
-            if p > 0:
-                arrive(hbuf.at[h, p, 0:BLK, 0:HALF], ("z", p, h))
-        if p == 0:
-            arrive(hbuf.at[other, 0, 0:BLK, 0:HALF], ("z", 0, 0), other)
-        else:
+    def route_a(p):
+        if p > 0:
             arrive(rslice(p, 0), ("zr", p))
-        for h in range(2):
-            ring_first(bslice, "b", "ab", p, h, hbuf)
         push(rslice(p, 0), rslice(p, 3), ("br", p, 3), dev(dx=1))
         push(rslice(p, 0), rslice(p, 1), ("br", p, 1), dev(dx=3))
 
-    def stage_b(p):
-        for h in range(2):
-            ring_forward(bslice, "b", "ab", p, h, hbuf)
+    def route_b(p):
         near, step = (3, 1) if p % 2 == 0 else (1, 3)
         arrive(rslice(p, near), ("br", p, near))
         push(rslice(p, near), rslice(p, 2), ("br", p, 2), dev(dx=step))
+
+    def route_c(p):
+        near = 3 if p % 2 == 0 else 1
         arrive(rslice(p, 4 - near), ("br", p, 4 - near))
-
-    def stage_c(p):
-        for h in range(2):
-            arrive(bslice(hbuf, p, h, 2), ("ab", p, h, 2))
-            ring_first(cslice, "c", "ac", p, h, hbuf)
         arrive(rslice(p, 2), ("br", p, 2))
 
-    def stage_d(p):
-        for h in range(2):
-            ring_forward(cslice, "c", "ac", p, h, hbuf)
-
-    def stage_e(p):
-        for h in range(2):
-            arrive(cslice(hbuf, p, h, 2), ("ac", p, h, 2))
+    def gather_a(p, h):
+        if p > 0:
+            arrive(hbuf.at[h, p, 0:BLK, 0:HALF], ("z", p, h))
+        elif h == 0:
+            arrive(hbuf.at[other, 0, 0:BLK, 0:HALF], ("zp",), other)
+        ring_first(bslice, "b", "ab", p, h, hbuf)
+
+    def gather_b(p, h):
+        ring_forward(bslice, "b", "ab", p, h, hbuf)
+
+    def gather_c(p, h):
+        ring_done(bslice, "ab", p, h, hbuf)
+        ring_first(cslice, "c", "ac", p, h, hbuf)
+
+    def gather_d(p, h):
+        ring_forward(cslice, "c", "ac", p, h, hbuf)
+
+    def gather_e(p, h):
+        ring_done(cslice, "ac", p, h, hbuf)
 
     def weight_ready(ks):
         for k in ks:
@@ -232,9 +270,8 @@
     def silu(v):
         return v / (1.0 + jnp.exp(-v))
 
-    def compute(g, planes):
-        first = g * planes
-        rows = planes * 64
+    def normalise(g):
+        first, planes = GROUPS_OF[g][0], len(GROUPS_OF[g])
         if g == 0:
             for o in range(NY):
                 for c in range(2):
@@ -244,7 +281,7 @@
             k = y * 2 + other
             arrive(gbuf.at[k], ("gain", 0), k)
 
-        def normalise(b, carry):
+        def block(b, carry):
             p = first + b // 4
             at = pl.ds(pl.multiple_of((b % 4) * BLK, BLK), BLK)
             to = pl.ds(pl.multiple_of(b * BLK, BLK), BLK)
@@ -261,7 +298,11 @@
                     hn[to, columns(h, r)] = (v * scale * gain).astype(BF16)
             return carry
 
-        lax.fori_loop(0, rows // BLK, normalise, 0)
+        lax.fori_loop(0, planes * 4, block, 0)
+
+    def hidden_units(g):
+        first, planes = GROUPS_OF[g][0], len(GROUPS_OF[g])
+        rows = planes * 64
         if g == 0:
             weight_ready(range(0, 4))
         route = rbuf[first : first + planes].reshape(rows, 128)
@@ -269,21 +310,24 @@
         for e in range(2):
             pick = jnp.where(pick_row == ep * 2 + e, 1.0, 0.0).astype(BF16)
             share = dot(route, pick)
-            gate = dot(hn[...], wgu[:, e * 256 : (e + 1) * 256])
-            up = dot(hn[...], wgu[:, 512 + e * 256 : 768 + e * 256])
-            inner[:, e * 256 : (e + 1) * 256] = (silu(gate) * up * share).astype(BF16)
+            gate = dot(hn[0:rows, :], wgu[:, e * 256 : (e + 1) * 256])
+            up = dot(hn[0:rows, :], wgu[:, 512 + e * 256 : 768 + e * 256])
+            inner[0:rows, e * 256 : (e + 1) * 256] = (silu(gate) * up * share).astype(BF16)
         if g == 0:
             weight_ready(range(4, 9))
             own = hn[0:BLK, :]
-            shared = (silu(dot(own, wsgu[:, 0:256])) * dot(own, wsgu[:, 256:512])).astype(BF16)
-        for h in range(2):
-            for r in range(NY):
-                part = dot(inner[...], wd[:, columns(h, r)])
-                cols = slice(r * HALF, (r + 1) * HALF)
-                pbuf[h, first : first + planes, :, cols] = part.reshape(planes, 64, HALF).astype(BF16)
-                if g == 0:
-                    extra = dot(shared, wsd[:, columns(h, r)])
-                    pbuf[h, 0, 0:BLK, cols] = (part[0:BLK] + extra).astype(BF16)
+            shared[...] = (silu(dot(own, wsgu[:, 0:256])) * dot(own, wsgu[:, 256:512])).astype(BF16)
+
+    def outputs(g, h):
+        first, planes = GROUPS_OF[g][0], len(GROUPS_OF[g])
+        rows = planes * 64
+        for r in range(NY):
+            part = dot(inner[0:rows, :], wd[:, columns(h, r)])
+            cols = slice(r * HALF, (r + 1) * HALF)
+            pbuf[h, first : first + planes, :, cols] = part.reshape(planes, 64, HALF).astype(BF16)
+            if g == 0:
+                extra = dot(shared[...], wsd[:, columns(h, r)])
+                pbuf[h, 0, 0:BLK, cols] = (part[0:BLK] + extra).astype(BF16)
 
     def land(stage, p, h, r):
         if stage == "b":
@@ -310,67 +354,56 @@
             mine[...].astype(F32) + land(stage, p, h, 1)[...].astype(F32) + land(stage, p, h, 3)[...].astype(F32)
         ).astype(BF16)
 
-    def stage_r1(p):
-        for h in range(2):
-            sum_first(cslice, "c", "rc", p, h)
-
-    def stage_r2(p):
-        for h in range(2):
-            sum_forward(cslice, "c", "rc", p, h)
-
-    def stage_r3(p):
-        for h in range(2):
-            sum_last(cslice, "c", "rc", p, h)
-            sum_first(bslice, "b", "rb", p, h)
-
-    def stage_r4(p):
-        for h in range(2):
-            sum_forward(bslice, "b", "rb", p, h)
-
-    def stage_r5(p):
-        for h in range(2):
-            sum_last(bslice, "b", "rb", p, h)
+    def sum_r(p, h):
+        sum_first(cslice, "c", "rc", p, h)
+
+    def sum_s(p, h):
+        sum_forward(cslice, "c", "rc", p, h)
+
+    def sum_t(p, h):
+        sum_last(cslice, "c", "rc", p, h)
+        sum_first(bslice, "b", "rb", p, h)
+
+    def sum_u(p, h):
+        sum_forward(bslice, "b", "rb", p, h)
+
+    def sum_w(p, h):
+        sum_last(bslice, "b", "rb", p, h)
         dz = SEQ[p]
         q = POS[(-dz) % NZ]
-        if p == 0:
+        if p > 0:
+            push(pbuf.at[h, p, 0:BLK, 0:HALF], zb.at[q, core], ("rz", q, 0), dev(dz=dz, c=h), core)
+        elif h == LAST_HALF:
             zb[0, core] = pbuf[core, 0, 0:BLK, 0:HALF]
-            push(pbuf.at[other, 0, 0:BLK, 0:HALF], zb.at[0, core], ("rz", 0, 0), dev(c=other), core)
-        else:
-            for h in range(2):
-                push(pbuf.at[h, p, 0:BLK, 0:HALF], zb.at[q, core], ("rz", q, 0), dev(dz=dz, c=h), core)
-
-    planes = 2
-    stages = (stage_a, stage_b, stage_c, stage_d, stage_e)
-    back = (stage_r2, stage_r3, stage_r4, stage_r5)
-    ready = {}
-    for tick in range(NZ + 4 + len(back)):
-        for k in range(len(back) - 1, -1, -1):
-            for p in range(NZ):
-                if ready.get(p) == tick - 1 - k:
-                    back[k](p)
-        for k in range(4, -1, -1):
-            if 0 <= tick - k < NZ:
-                stages[k](tick - k)
-        last = tick - 4
-        if 0 <= last < NZ and (last + 1) % planes == 0:
-            g = last // planes
-            compute(g, planes)
-            for p in range(g * planes, (g + 1) * planes):
-                stage_r1(p)
-                ready[p] = tick
-
-    for p in range(1, NZ):
-        for c in range(2):
-            arrive(zb.at[p, c], ("rz", p, c))
-    arrive(zb.at[0, other], ("rz", 0, 0), other)
+            push(pbuf.at[other, 0, 0:BLK, 0:HALF], zb.at[0, core], ("rzp",), dev(c=other), core)
+
+    steps = dict(i=route_a, j=route_b, k=route_c, a=gather_a, b=gather_b, c=gather_c, d=gather_d, e=gather_e)
+    steps |= dict(n=normalise, m=hidden_units, v=outputs, r=sum_r, s=sum_s, t=sum_t, u=sum_u, w=sum_w)
+    for name in ORDER:
+        with jax.named_scope(name):
+            steps[name[0]](*[int(digit) for digit in name[1:]])
+
+    with jax.named_scope("final"):
+        for p in range(1, NZ):
+            for c in range(2):
+                arrive(zb.at[p, c], ("rz", p, c))
+        arrive(zb.at[0, other], ("rzp",), other)
+    live = live_slots((2 * BLK, HALF), 0)
     for c in range(2):
         total = zb[0, c].astype(F32)
         for p in range(1, NZ):
             total = total + zb[p, c].astype(F32)
-        alive = live[c * BLK : (c + 1) * BLK, 0:1]
+        alive = live[c * BLK : (c + 1) * BLK]
         out_ref[c] = jnp.where(alive, total, 0.0).astype(BF16)
-    for cp in started:
-        cp.wait_send()
+    with jax.named_scope("drain"):
+        rings = {"ab0": fb.at[0], "ab1": fb.at[1], "ac0": fc0, "ac1": fc1}
+        rings |= {"rb0": fb.at[0], "rb1": fb.at[1], "rc0": fc0, "rc1": fc1}
+        rings |= {"z": zb.at[1:NZ], "zp": zb.at[0, 0], "rz": zb.at[1:NZ], "rzp": zb.at[0, 0]}
+        rings |= {"zr": rbuf.at[0:7, 0:BLK, :], "br": rbuf.at[:, 0:48, :], "gain": gbuf.at[0:7]}
+        for name, ref in rings.items():
+            sent(ref, ssem.at[GROUPS.index(name)])
+        for k, (s, _) in enumerate(weights):
+            sent(s, wsem.at[k])
 
 
 def body(hidden, norm_gain, expert_ids, route_weights, lengths, gate_proj, up_proj, down_proj, sgate, sup, sdown):
@@ -390,6 +423,7 @@
             pltpu.VMEM((8, 1, HALF), F32),
             pltpu.VMEM((128, 4096), BF16),
             pltpu.VMEM((128, 512), BF16),
+            pltpu.VMEM((BLK, 256), BF16),
             pltpu.VMEM((4096, 1024), BF16),
             pltpu.VMEM((512, 4096), BF16),
             pltpu.VMEM((4096, 512), BF16),
@@ -399,7 +433,8 @@
             pltpu.VMEM((2, NZ, 3, BLK, HALF), BF16),
             pltpu.VMEM((NZ, 2, BLK, HALF), BF16),
             pltpu.SemaphoreType.DMA((9,)),
-            pltpu.SemaphoreType.DMA((n,)),
+            pltpu.SemaphoreType.DMA((9,)),
+            pltpu.SemaphoreType.DMA((len(GROUPS),)),
             pltpu.SemaphoreType.DMA((n,)),
         ],
         compiler_params=pltpu.CompilerParams(
@@ -408,8 +443,8 @@
     )(
         hidden.reshape(2, BLK, HALF),
         norm_gain.reshape(1, HALF),
-        expert_ids,
-        route_weights,
+        expert_ids.T,
+        route_weights.T,
         lengths,
         gate_proj,
         up_proj,

time: 106 us -> 76.8 us (0.72)
  Pallas kernels: 101 us -> 75.2 us
  local copies, waits for them, and re-layouts: 4.1 us -> 1.38 us
    pallas_call x1, Pallas kernels: 101 us -> 75.2 us  [body(): pl.pallas_call(kernel, out_shape=jax.ShapeDtypeStruct((2, BLK, HALF), BF1...]
    unnamed x3 -> x1, local copies, waits for them, and re-layouts: 4.1 us -> 1.38 us
where the time goes in v2:
time: 76.8 us; the launch traced here: 76.6 us
  Pallas kernels  75.2 us (98%)
  local copies, waits for them, and re-layouts  1.38 us (2%)
    pallas_call x1, Pallas kernels, body(): pl.pallas_call(kernel, out_shape=jax.ShapeDtypeStruct((2, BLK, HALF), BF1...  75.2 us

profile of v2, /device:TPU:1, one launch (start us, length us, event | category | flops | bytes accessed | tf_op | source)
XLA Modules:
  0.0 76.6 jit_solution(17776192426298692613)
XLA Ops:
  0.0 75.2 %shard_map.109 = bf16[2,16,512]{2,1,0:T(8,128)(2,1)} custom-call(bf16[2,16,512]{2,1,0:T(8,128)(2,1)} %bitcast.6, f32[1,512]{1,0:T(1,128)} %bitcast.9, s32[8,32]{1,0:T(8,128)} %bitcast.7, f32[8,32]{1,0:T(8,128)} %bitcast.8, s32[4]{0:T(128)} %len_ref.1, bf16[2,4096,128]{2,1,0:T(8,128)(2,1)} %gate_ref.1, bf16[2,4096,128]{2,1,0:T(8,128)(2,1)} %up_ref.1, ...), custom_call_target="tpu_custom_call" | custom-call | tf_op jit(solution)/shard_map/pallas_call | solution.py:413
  75.2 1.4 %copy.13 = bf16[32,512]{1,0:T(8,128)(2,1)} copy(bf16[32,512]{1,0:T(8,128)(2,1)} %bitcast.5) | data formatting | bytes 65536

commit v3 on v2

v3 whole, which is shorter than its diff:
```python
import functools

import jax
import jax.numpy as jnp
from jax import lax
from jax.experimental import pallas as pl
from jax.experimental.pallas import tpu as pltpu
from jax.sharding import PartitionSpec as P

MESH = pl.DeviceIdType.MESH
EPS = 1e-06
NZ, NX, NY = 8, 4, 4
BLK = 16
HALF = 512
F32, BF16 = jnp.float32, jnp.bfloat16
SEQ = (0, 1, 7, 2, 6, 3, 5, 4)
POS = {dz: i for i, dz in enumerate(SEQ)}


GROUPS_OF = ((0, 3), (4, 5), (1, 2), (6, 7))
ORDER = (
    "i0", "a00", "a01", "j0", "i1", "b00", "b01", "i2", "c00", "c01", "k0", "a31", "a30", "i3", "j1", "a40",
    "a41", "a50", "a51", "i4", "i5", "j2", "i6", "a61", "a60", "d00", "a71", "d01", "a70", "i7", "b31", "b30",
    "j3", "k1", "b50", "b51", "j5", "b40", "b41", "c31", "c30", "j4", "k2", "b60", "j6", "c40", "c41", "b71",
    "b70", "j7", "b61", "k3", "c50", "e01", "c51", "k5", "e00", "d31", "d30", "c60", "k4", "k6", "c70", "d41",
    "c71", "k7", "d40", "c61", "d51", "d50", "e11", "e21", "e31", "e30", "n0", "m0", "v01", "r31", "v00", "r30",
    "e20", "d60", "d71", "e10", "e41", "e40", "d70", "n2", "e50", "d61", "m2", "v20", "v21", "e51", "n1", "s31",
    "s30", "m1", "v10", "r40", "v11", "r41", "r51", "r50", "e70", "e61", "e71", "e60", "n3", "m3", "t30", "t31",
    "v30", "r60", "r70", "v31", "r71", "s40", "r61", "q03", "q01", "s41", "q02", "r00", "q00", "s50", "s51", "q12",
    "u31", "w31", "u30", "w30", "q13", "r01", "s71", "s60", "q11", "s70", "s61", "q10", "t51", "t40", "t41", "t50",
    "s00", "s01", "t70", "t71", "t60", "t61", "u51", "w51", "u40", "w40", "u41", "w41", "u50", "w50", "t00", "t01",
    "u71", "w71", "u70", "w70", "u61", "w61", "u60", "w60", "u00", "w00", "u01", "w01",
)
RELAYED = (1, 2)
DIRECT_OUT = (0, 3, 4)
DIRECT_BACK = (0, 3, 4, 5, 6, 7)
PLANES = tuple(p for p in range(8) if p not in RELAYED)
FIRST_HALF = 0 if ORDER.index("a00") < ORDER.index("a01") else 1
LAST_HALF = 1 if ORDER.index("w00") < ORDER.index("w01") else 0


def shared_key(key):
    if key[0] in ("ab", "ac"):
        return key if key[3] == (3 if key[1] % 2 == 0 else 1) else key[:3] + (2,)
    if key[0] in ("rb", "rc"):
        direct = key[0] == "rb" and key[1] in DIRECT_BACK
        return key[:3] + (1,) if direct or key[3] != 2 else key
    if key[0] == "br":
        return key if key[2] == (3 if key[1] % 2 == 0 else 1) else key[:2] + (2,)
    if key[0] == "rz":
        return ("rz",)
    return key


class Ids:
    def __init__(self):
        self.table, self.count = {}, 0

    def at(self, *key):
        key = shared_key(key)
        if key not in self.table:
            self.table[key] = self.count
            self.count += 1
        return self.table[key]


def build_ids():
    ids = Ids()
    ids.count = ids.at("zp") + 2
    for p in range(NZ):
        for h in range(2):
            ids.at("z", p, h)
    for p in range(NZ):
        ids.at("zr", p)
        for r in (1, 2, 3):
            ids.at("br", p, r)
            for h in range(2):
                for stage in ("ab", "ac", "rc", "rb"):
                    ids.at(stage, p, h, r)
    for name in ("rz", "rzp", "gain"):
        ids.at(name)
    for p in RELAYED:
        for h in range(2):
            ids.at("zf", p, h)
            for r in range(4):
                ids.at("zs", r, h, p)
    for k in range(9):
        ids.at("w", k)
    return ids


IDS = build_ids()
RINGS = ("ab", "ac", "rb", "rc")
GROUPS = [k + str(h) for k in RINGS for h in range(2)] + ["z", "zp", "zr", "br", "gain", "rz", "rzp", "w", "zf", "zs0", "zs1"]


def kernel(
    hidden_in, gain_in, eid_in, rw_in, len_ref, gate_ref, up_ref, down_ref, sgate_ref, sup_ref, sdown_ref,
    out_ref,
    hbuf, pbuf, rbuf, rown, gbuf, hn, inner, shared, wgu, wd, wsgu, wsd, fc0, fc1, fb, zb, zsum, hidden_ref, eid_ref, rw_ref, isem, lsem, wsem, ssem, rsem,
):
    ep, tp = lax.axis_index("ep"), lax.axis_index("tp")
    z, x = ep // NX, ep % NX
    y, core = tp // 2, tp % 2
    other = 1 - core

    def dev(dz=0, dx=0, dy=0, c=None):
        c = core if c is None else c
        return (((z + dz) % NZ) * NX + (x + dx) % NX, ((y + dy) % NY) * 2 + c)

    barrier = pltpu.get_barrier_semaphore()
    peers = [dev(dz=o, c=c) for o in range(1, NZ) for c in range(2)] + [dev(c=other)]
    peers += [dev(dy=o, c=c) for o in range(1, NY) for c in range(2)]
    peers += [dev(dx=o) for o in range(1, NX)]
    for peer in peers:
        pl.semaphore_signal(barrier, inc=1, device_id=peer, device_id_type=MESH)

    inputs = [
        pltpu.make_async_copy(eid_in, eid_ref, isem.at[0]),
        pltpu.make_async_copy(rw_in, rw_ref, isem.at[1]),
        pltpu.make_async_copy(hidden_in, hidden_ref, isem.at[2]),
        pltpu.make_async_copy(hidden_in.at[core], hbuf.at[core, 0, 0:BLK, 0:HALF], isem.at[3]),
        pltpu.make_async_copy(gain_in, gbuf.at[tp], isem.at[4]),
    ]
    for cp in inputs:
        cp.start()

    def group(key):
        return GROUPS.index(key[0] + str(key[2]) if key[0] in RINGS + ("zs",) else key[0])

    def push(src, dst, key, to, add=0):
        i = IDS.at(*key) + add
        sem = ssem.at[group(key)]
        if key[0] == "w":
            sem = wsem.at[key[1]]
        pltpu.make_async_remote_copy(
            src_ref=src, dst_ref=dst, send_sem=sem, recv_sem=rsem.at[i], device_id=to, device_id_type=MESH
        ).start()

    def sent(ref, sem):
        pltpu.make_async_remote_copy(
            src_ref=ref, dst_ref=ref, send_sem=sem, recv_sem=rsem.at[0], device_id=dev(c=other), device_id_type=MESH
        ).wait_send()

    def arrive(dst, key, add=0):
        i = IDS.at(*key) + add
        pltpu.make_async_remote_copy(
            src_ref=dst, dst_ref=dst, send_sem=ssem.at[0], recv_sem=rsem.at[i], device_id=dev(c=other), device_id_type=MESH
        ).wait_recv()

    def lanes(first):
        return pl.ds(pl.multiple_of(first + core * 128, 128), 128)

    weights = []
    for e in range(2):
        weights.append((gate_ref.at[e], wgu.at[:, lanes(e * 256)]))
        weights.append((up_ref.at[e], wgu.at[:, lanes(512 + e * 256)]))
    weights.append((sgate_ref, wsgu.at[:, lanes(0)]))
    weights.append((sup_ref, wsgu.at[:, lanes(256)]))
    for e in range(2):
        weights.append((down_ref.at[e], wd.at[lanes(e * 256), :]))
    weights.append((sdown_ref, wsd.at[lanes(0), :]))
    local = [pltpu.make_async_copy(s, d, lsem.at[k]) for k, (s, d) in enumerate(weights)]
    for cp in local:
        cp.start()

    def live_slots(shape, dim):
        slot = lax.broadcasted_iota(jnp.int32, shape, dim)
        seq_len = jnp.zeros(shape, jnp.int32)
        for q in range(4):
            seq_len = jnp.where(slot // 8 == q, len_ref[q], seq_len)
        return slot % 8 < seq_len

    for cp in inputs:
        cp.wait()
    expert = lax.broadcasted_iota(jnp.int32, (128, 32), 0)
    mix = jnp.zeros((128, 32), F32)
    for k in range(8):
        mix = mix + jnp.where(eid_ref[k : k + 1, :] == expert % 64, rw_ref[k : k + 1, :], 0.0)
    mix = jnp.where(live_slots((128, 32), 1), mix, 0.0)
    high = mix.astype(BF16).astype(F32)
    terms = jnp.where(expert < 64, high, mix - high).T
    rown[...] = terms.reshape(2, BLK, 128).astype(BF16)
    rbuf[0, 0:BLK, :] = rown[core]

    with jax.named_scope("barrier"):
        pl.semaphore_wait(barrier, len(peers))

    for o in (1, 7, 2, 6, 3, 5, 4):
        p = POS[(-o) % NZ]
        if o == 1:
            push(hidden_ref.at[other], hbuf.at[core, 0, 0:BLK, 0:HALF], ("zp",), dev(c=other), core)
        if p not in RELAYED:
            for c in range(2):
                push(hidden_ref.at[c], hbuf.at[core, p, 0:BLK, 0:HALF], ("z", p, 0), dev(dz=o, c=c), core)
        push(rown.at[core], rbuf.at[p, 0:BLK, :], ("zr", p), dev(dz=o))
    for k, (s, d) in enumerate(weights):
        if k < 4:
            push(s, d, ("w", k), dev(c=other))
    for o in range(NY):
        for c in range(2):
            if o > 0:
                push(gbuf.at[tp], gbuf.at[tp], ("gain",), dev(dy=o, c=c))
    push(gbuf.at[tp], gbuf.at[tp], ("gain",), dev(c=other))
    for k, (s, d) in enumerate(weights):
        if k >= 4:
            push(s, d, ("w", k), dev(c=other))

    def bslice(ref, p, h, r):
        if h == 0:
            return ref.at[h, p, 0:BLK, r * HALF : (r + 1) * HALF]
        return ref.at[h, p, r * BLK : (r + 1) * BLK, 0:HALF]

    def cslice(ref, p, h, r):
        if h == 0:
            return ref.at[h, p, r * BLK : (r + 1) * BLK, :]
        return ref.at[h, p, :, r * HALF : (r + 1) * HALF]

    def pair(view, ref, p, h):
        if view is bslice:
            return ref.at[h, p, 0 : 2 * BLK, 0:HALF] if h == 1 else ref.at[h, p, 0:BLK, 0 : 2 * HALF]
        return ref.at[h, p, 0 : 2 * BLK, :] if h == 0 else ref.at[h, p, :, 0 : 2 * HALF]

    def along(stage, h, step):
        on_y = (stage == "b") == (h == 0)
        return dev(dy=step % NY) if on_y else dev(dx=step % NX)

    def ring_first(view, stage, key, p, h, ref):
        push(view(ref, p, h, 0), view(ref, p, h, 3), (key, p, h, 3), along(stage, h, 1))
        push(view(ref, p, h, 0), view(ref, p, h, 1), (key, p, h, 1), along(stage, h, -1))
        if stage == "b" and p in DIRECT_OUT:
            push(view(ref, p, h, 0), view(ref, p, h, 2), (key, p, h, 2), along(stage, h, 2))

    def ring_forward(view, stage, key, p, h, ref):
        near, step = (3, 1) if p % 2 == 0 else (1, -1)
        arrive(view(ref, p, h, near), (key, p, h, near))
        if stage == "c" or p not in DIRECT_OUT:
            push(view(ref, p, h, near), view(ref, p, h, 2), (key, p, h, 2), along(stage, h, step))

    def ring_done(view, key, p, h, ref):
        arrive(pair(view, ref, p, h), (key, p, h, 2))

    def rslice(p, r):
        return rbuf.at[p, r * BLK : (r + 1) * BLK, :]

    def route_a(p):
        if p > 0:
            arrive(rslice(p, 0), ("zr", p))
        push(rslice(p, 0), rslice(p, 3), ("br", p, 3), dev(dx=1))
        push(rslice(p, 0), rslice(p, 1), ("br", p, 1), dev(dx=3))

    def route_b(p):
        near, step = (3, 1) if p % 2 == 0 else (1, 3)
        arrive(rslice(p, near), ("br", p, near))
        push(rslice(p, near), rslice(p, 2), ("br", p, 2), dev(dx=step))

    def route_c(p):
        arrive(rbuf.at[p, 0 : 2 * BLK, :], ("br", p, 2))

    def gather_a(p, h):
        if p > 0:
            arrive(hbuf.at[h, p, 0:BLK, 0:HALF], ("z", p, h))
        elif h == FIRST_HALF:
            arrive(hbuf.at[other, 0, 0:BLK, 0:HALF], ("zp",), other)
        ring_first(bslice, "b", "ab", p, h, hbuf)

    def gather_b(p, h):
        ring_forward(bslice, "b", "ab", p, h, hbuf)

    def relay(h, slots):
        for p in RELAYED:
            for r in slots:
                push(cslice(hbuf, 0, h, r), cslice(hbuf, p, h, r), ("zf", p, h), dev(dz=-SEQ[p] % NZ))

    def gather_c(p, h):
        ring_done(bslice, "ab", p, h, hbuf)
        ring_first(cslice, "c", "ac", p, h, hbuf)
        if p == 0:
            relay(h, (0,))

    def gather_d(p, h):
        ring_forward(cslice, "c", "ac", p, h, hbuf)
        if p == 0:
            relay(h, (3,))

    def gather_e(p, h):
        if p in RELAYED:
            arrive(hbuf.at[h, p], ("zf", p, h))
            return
        ring_done(cslice, "ac", p, h, hbuf)
        if p == 0:
            relay(h, (1, 2))

    def weight_ready(ks):
        for k in ks:
            local[k].wait()
            arrive(partner[k], ("w", k))

    def plan_partner():
        def lo(first):
            return pl.ds(pl.multiple_of(first + other * 128, 128), 128)

        out = []
        for e in range(2):
            out += [wgu.at[:, lo(e * 256)], wgu.at[:, lo(512 + e * 256)]]
        out += [wsgu.at[:, lo(0)], wsgu.at[:, lo(256)]]
        out += [wd.at[lo(e * 256), :] for e in range(2)]
        return out + [wsd.at[lo(0), :]]

    partner = plan_partner()

    def dot(a, b):
        return jnp.dot(a, b, preferred_element_type=F32)

    def columns(h, r):
        return pl.ds(pl.multiple_of(((y + r) % NY) * 1024 + h * HALF, HALF), HALF)

    def silu(v):
        return v / (1.0 + jnp.exp(-v))

    def normalise(g):
        low, high = GROUPS_OF[g]
        if g == 0:
            arrive(gbuf.at[0:7], ("gain",))

        def block(b, carry):
            p = low + (b // 4) * (high - low)
            at = pl.ds(pl.multiple_of((b % 4) * BLK, BLK), BLK)
            to = pl.ds(pl.multiple_of(b * BLK, BLK), BLK)
            squares = jnp.zeros((BLK, HALF), F32)
            for h in range(2):
                for r in range(NY):
                    v = hbuf[h, p, at, r * HALF : (r + 1) * HALF].astype(F32)
                    squares = squares + v * v
            scale = lax.rsqrt(jnp.sum(squares, axis=1, keepdims=True) / 4096.0 + EPS)
            for h in range(2):
                for r in range(NY):
                    v = hbuf[h, p, at, r * HALF : (r + 1) * HALF].astype(F32)
                    gain = gbuf[((y + r) % NY) * 2 + h]
                    hn[to, columns(h, r)] = (v * scale * gain).astype(BF16)
            return carry

        lax.fori_loop(0, 8, block, 0)

    def hidden_units(g):
        if g == 0:
            weight_ready(range(0, 4))
        route = jnp.concatenate([rbuf[p] for p in GROUPS_OF[g]], axis=0)
        pick_row = lax.broadcasted_iota(jnp.int32, (128, 256), 0) % 64
        for e in range(2):
            pick = jnp.where(pick_row == ep * 2 + e, 1.0, 0.0).astype(BF16)
            share = dot(route, pick)
            gate = dot(hn[...], wgu[:, e * 256 : (e + 1) * 256])
            up = dot(hn[...], wgu[:, 512 + e * 256 : 768 + e * 256])
            inner[:, e * 256 : (e + 1) * 256] = (silu(gate) * up * share).astype(BF16)
        if g == 0:
            weight_ready(range(4, 9))
            own = hn[0:BLK, :]
            shared[...] = (silu(dot(own, wsgu[:, 0:256])) * dot(own, wsgu[:, 256:512])).astype(BF16)

    def outputs(g, h):
        for r in range(NY):
            part = dot(inner[...], wd[:, columns(h, r)])
            cols = slice(r * HALF, (r + 1) * HALF)
            for n, p in enumerate(GROUPS_OF[g]):
                pbuf[h, p, :, cols] = part[n * 64 : (n + 1) * 64].astype(BF16)
                if p == 0:
                    extra = dot(shared[...], wsd[:, columns(h, r)])
                    pbuf[h, 0, 0:BLK, cols] = (part[0:BLK] + extra).astype(BF16)
        for p in GROUPS_OF[g]:
            if p in RELAYED:
                for r in (2, 3, 1, 0):
                    push(cslice(pbuf, p, h, r), cslice(zsum, p - 1, h, r), ("zs", r, h, p), dev(dz=SEQ[p]))

    def relayed(h, r):
        for p in RELAYED:
            arrive(cslice(zsum, p - 1, h, r), ("zs", r, h, p))
        mine = cslice(pbuf, 0, h, r)
        total = mine[...].astype(F32)
        for p in RELAYED:
            total = total + cslice(zsum, p - 1, h, r)[...].astype(F32)
        mine[...] = total.astype(BF16)

    def land(stage, p, h, r):
        if stage == "b":
            return fb.at[h, p, r - 1]
        return (fc0 if h == 0 else fc1).at[p, r - 1]

    def sum_first(view, stage, key, p, h):
        near, step = (1, 1) if p % 2 == 0 else (3, -1)
        if stage == "b" and p in DIRECT_BACK:
            for r in (2, 1, 3):
                push(view(pbuf, p, h, r), land(stage, p, h, 4 - r), (key, p, h, 1), along(stage, h, r))
            return
        push(view(pbuf, p, h, 2), land(stage, p, h, 2), (key, p, h, 2), along(stage, h, step))
        push(view(pbuf, p, h, 4 - near), land(stage, p, h, near), (key, p, h, near), along(stage, h, -step))

    def sum_forward(view, stage, key, p, h):
        near, step = (1, 1) if p % 2 == 0 else (3, -1)
        if stage == "b" and p in DIRECT_BACK:
            return
        arrive(land(stage, p, h, 2), (key, p, h, 2))
        mine = view(pbuf, p, h, near)
        mine[...] = (mine[...].astype(F32) + land(stage, p, h, 2)[...].astype(F32)).astype(BF16)
        push(mine, land(stage, p, h, 4 - near), (key, p, h, 4 - near), along(stage, h, step))

    def sum_last(view, stage, key, p, h):
        whole = fb.at[h, p] if stage == "b" else (fc0 if h == 0 else fc1).at[p]
        direct = stage == "b" and p in DIRECT_BACK
        arrive(whole if direct else whole.at[0:2], (key, p, h, 1))
        mine = view(pbuf, p, h, 0)
        total = mine[...].astype(F32)
        for r in (1, 2, 3) if direct else (1, 3):
            total = total + land(stage, p, h, r)[...].astype(F32)
        mine[...] = total.astype(BF16)

    def sum_r(p, h):
        sum_first(cslice, "c", "rc", p, h)

    def sum_s(p, h):
        sum_forward(cslice, "c", "rc", p, h)

    def sum_t(p, h):
        sum_last(cslice, "c", "rc", p, h)
        sum_first(bslice, "b", "rb", p, h)

    def sum_u(p, h):
        sum_forward(bslice, "b", "rb", p, h)

    def sum_w(p, h):
        sum_last(bslice, "b", "rb", p, h)
        dz = SEQ[p]
        q = POS[(-dz) % NZ]
        if p > 0:
            push(pbuf.at[h, p, 0:BLK, 0:HALF], zb.at[q, core], ("rz",), dev(dz=dz, c=h))
        elif h == LAST_HALF:
            zb[0, core] = pbuf[core, 0, 0:BLK, 0:HALF]
            push(pbuf.at[other, 0, 0:BLK, 0:HALF], zb.at[0, core], ("rzp",), dev(c=other))

    steps = dict(i=route_a, j=route_b, k=route_c, a=gather_a, b=gather_b, c=gather_c, d=gather_d, e=gather_e)
    steps |= dict(n=normalise, m=hidden_units, v=outputs, q=relayed, r=sum_r, s=sum_s, t=sum_t, u=sum_u, w=sum_w)
    for name in ORDER:
        with jax.named_scope(name):
            steps[name[0]](*[int(digit) for digit in name[1:]])

    with jax.named_scope("final"):
        arrive(zb.at[1 : len(PLANES)], ("rz",))
        arrive(zb.at[0, other], ("rzp",))
    live = live_slots((2 * BLK, HALF), 0)
    for c in range(2):
        total = zb[0, c].astype(F32)
        for p in PLANES[1:]:
            total = total + zb[p, c].astype(F32)
        alive = live[c * BLK : (c + 1) * BLK]
        out_ref[c] = jnp.where(alive, total, 0.0).astype(BF16)
    with jax.named_scope("drain"):
        n = len(PLANES)
        rings = {"zp": zb.at[0, 0], "rzp": zb.at[0, 0], "z": zb.at[1:n], "rz": zb.at[1:n]}
        rings |= {"zr": rbuf.at[0:7, 0:BLK, :], "br": rbuf.at[:, 0:48, :], "gain": gbuf.at[0:7]}
        for h in range(2):
            rings |= {f"ab{h}": fb.at[h, 0:n], f"rb{h}": fb.at[h, 0:n]}
            rings |= {f"ac{h}": (fc0, fc1)[h].at[0:n], f"rc{h}": (fc0, fc1)[h].at[0:n]}
            if RELAYED:
                rings[f"zs{h}"] = hbuf.at[h, 0 : len(RELAYED)]
        if RELAYED:
            rings["zf"] = hbuf.at[:, 0 : len(RELAYED)]
        for name, ref in rings.items():
            sent(ref, ssem.at[GROUPS.index(name)])
        for k, (s, _) in enumerate(weights):
            sent(s, wsem.at[k])


def body(hidden, norm_gain, expert_ids, route_weights, lengths, gate_proj, up_proj, down_proj, sgate, sup, sdown):
    vmem = pl.BlockSpec(memory_space=pltpu.VMEM)
    anywhere = pl.BlockSpec(memory_space=pl.ANY)
    n = IDS.count
    out = pl.pallas_call(
        kernel,
        out_shape=jax.ShapeDtypeStruct((2, BLK, HALF), BF16),
        in_specs=[anywhere] * 4 + [pl.BlockSpec(memory_space=pltpu.SMEM)] + [anywhere] * 6,
        out_specs=vmem,
        scratch_shapes=[
            pltpu.VMEM((2, NZ, 64, 2048), BF16),
            pltpu.VMEM((2, NZ, 64, 2048), BF16),
            pltpu.VMEM((NZ, 64, 128), BF16),
            pltpu.VMEM((2, BLK, 128), BF16),
            pltpu.VMEM((8, 1, HALF), F32),
            pltpu.VMEM((128, 4096), BF16),
            pltpu.VMEM((128, 512), BF16),
            pltpu.VMEM((BLK, 256), BF16),
            pltpu.VMEM((4096, 1024), BF16),
            pltpu.VMEM((512, 4096), BF16),
            pltpu.VMEM((4096, 512), BF16),
            pltpu.VMEM((256, 4096), BF16),
            pltpu.VMEM((NZ, 3, BLK, 2048), BF16),
            pltpu.VMEM((NZ, 3, 64, HALF), BF16),
            pltpu.VMEM((2, NZ, 3, BLK, HALF), BF16),
            pltpu.VMEM((NZ, 2, BLK, HALF), BF16),
            pltpu.VMEM((2, 2, 64, 2048), BF16),
            pltpu.VMEM((2, BLK, HALF), BF16),
            pltpu.VMEM((8, 32), jnp.int32),
            pltpu.VMEM((8, 32), F32),
            pltpu.SemaphoreType.DMA((5,)),
            pltpu.SemaphoreType.DMA((9,)),
            pltpu.SemaphoreType.DMA((9,)),
            pltpu.SemaphoreType.DMA((len(GROUPS),)),
            pltpu.SemaphoreType.DMA((n,)),
        ],
        compiler_params=pltpu.CompilerParams(
            collective_id=0, has_side_effects=True, vmem_limit_bytes=60 * 1024 * 1024
        ),
    )(
        hidden.reshape(2, BLK, HALF),
        norm_gain.reshape(1, HALF),
        expert_ids.T,
        route_weights.T,
        lengths,
        gate_proj,
        up_proj,
        down_proj,
        sgate,
        sup,
        sdown,
    )
    return out.reshape(2 * BLK, HALF)


def solution(mesh):
    placed = (
        P("ep", "tp"),
        P("tp"),
        P("ep", None),
        P("ep", None),
        P("ep"),
        P("ep", None, "tp"),
        P("ep", None, "tp"),
        P("ep", "tp", None),
        P(None, "tp"),
        P(None, "tp"),
        P("tp", None),
    )
    return jax.shard_map(body, mesh=mesh, in_specs=placed, out_specs=P("ep", "tp"), check_vma=False)
```

time: 76.8 us -> 67.9 us (0.88)
  Pallas kernels: 75.2 us -> 66.4 us
    pallas_call x1, Pallas kernels: 75.2 us -> 66.4 us  [body(): pl.pallas_call(kernel, out_shape=jax.ShapeDtypeStruct((2, BLK, HALF), BF1...]
where the time goes in v3:
time: 67.9 us; the launch traced here: 67.8 us
  Pallas kernels  66.4 us (98%)
  local copies, waits for them, and re-layouts  1.38 us (2%)
    pallas_call x1, Pallas kernels, body(): pl.pallas_call(kernel, out_shape=jax.ShapeDtypeStruct((2, BLK, HALF), BF1...  66.4 us
    unnamed x1, local copies, waits for them, and re-layouts  1.38 us

profile of v3, /device:TPU:1, one launch (start us, length us, event | category | flops | bytes accessed | tf_op | source)
XLA Modules:
  0.0 67.8 jit_solution(14346634484219471920)
XLA Ops:
  0.0 66.4 %shard_map.109 = bf16[2,16,512]{2,1,0:T(8,128)(2,1)} custom-call(bf16[2,16,512]{2,1,0:T(8,128)(2,1)} %bitcast.6, f32[1,512]{1,0:T(1,128)} %bitcast.9, s32[8,32]{1,0:T(8,128)} %bitcast.7, f32[8,32]{1,0:T(8,128)} %bitcast.8, s32[4]{0:T(128)} %len_ref.1, bf16[2,4096,128]{2,1,0:T(8,128)(2,1)} %gate_ref.1, bf16[2,4096,128]{2,1,0:T(8,128)(2,1)} %up_ref.1, ...), custom_call_target="tpu_custom_call" | custom-call | tf_op jit(solution)/shard_map/pallas_call | solution.py:477
  66.4 1.4 %copy.13 = bf16[32,512]{1,0:T(8,128)(2,1)} copy(bf16[32,512]{1,0:T(8,128)(2,1)} %bitcast.5) | data formatting | bytes 65536

commit v4 on v3

--- a/solution.py
+++ b/solution.py
@@ -19,21 +19,22 @@
 
 GROUPS_OF = ((0, 3), (4, 5), (1, 2), (6, 7))
 ORDER = (
-    "i0", "a00", "a01", "j0", "i1", "b00", "b01", "i2", "c00", "c01", "k0", "a31", "a30", "i3", "j1", "a40",
-    "a41", "a50", "a51", "i4", "i5", "j2", "i6", "a61", "a60", "d00", "a71", "d01", "a70", "i7", "b31", "b30",
-    "j3", "k1", "b50", "b51", "j5", "b40", "b41", "c31", "c30", "j4", "k2", "b60", "j6", "c40", "c41", "b71",
-    "b70", "j7", "b61", "k3", "c50", "e01", "c51", "k5", "e00", "d31", "d30", "c60", "k4", "k6", "c70", "d41",
-    "c71", "k7", "d40", "c61", "d51", "d50", "e11", "e21", "e31", "e30", "n0", "m0", "v01", "r31", "v00", "r30",
-    "e20", "d60", "d71", "e10", "e41", "e40", "d70", "n2", "e50", "d61", "m2", "v20", "v21", "e51", "n1", "s31",
-    "s30", "m1", "v10", "r40", "v11", "r41", "r51", "r50", "e70", "e61", "e71", "e60", "n3", "m3", "t30", "t31",
-    "v30", "r60", "r70", "v31", "r71", "s40", "r61", "q03", "q01", "s41", "q02", "r00", "q00", "s50", "s51", "q12",
-    "u31", "w31", "u30", "w30", "q13", "r01", "s71", "s60", "q11", "s70", "s61", "q10", "t51", "t40", "t41", "t50",
-    "s00", "s01", "t70", "t71", "t60", "t61", "u51", "w51", "u40", "w40", "u41", "w41", "u50", "w50", "t00", "t01",
-    "u71", "w71", "u70", "w70", "u61", "w61", "u60", "w60", "u00", "w00", "u01", "w01",
+    "a00", "a01", "y", "b01", "b00", "c00", "c01", "a31", "a30", "a50", "i5", "i2", "i4", "i3", "a41", "a40",
+    "a61", "a60", "a51", "i0", "i6", "i1", "d01", "a71", "a70", "b30", "d00", "i7", "b41", "b31", "c31", "c30",
+    "b51", "c41", "b50", "j6", "b71", "b70", "b40", "j3", "j4", "j7", "c40", "j5", "j2", "b60", "e01", "b61",
+    "e00", "n0", "j1", "d31", "d30", "j0", "c50", "c51", "c60", "k3", "k5", "d40", "c61", "x", "c70", "e11",
+    "k1", "k4", "e21", "d41", "k0", "c71", "k7", "k2", "k6", "e31", "e30", "n3", "m01", "m00", "d50", "d51",
+    "v00", "e10", "v01", "e20", "n1", "r31", "r30", "d60", "n2", "d61", "m21", "d70", "d71", "m20", "e40", "v21",
+    "v20", "e41", "e51", "e50", "n4", "n5", "m10", "s31", "m11", "v11", "r41", "v10", "r50", "r51", "e71", "e60",
+    "e61", "e70", "n7", "n6", "r40", "m30", "m31", "v31", "r71", "t31", "v30", "r70", "r61", "q11", "s41", "s50",
+    "s30", "r60", "s51", "q13", "s40", "q12", "s71", "r01", "q02", "q03", "s70", "r00", "s61", "u31", "s60", "t50",
+    "t41", "t51", "q01", "t30", "t40", "t71", "s01", "s00", "t70", "q10", "t60", "t61", "u40", "u41", "u51", "u50",
+    "w50", "u30", "t01", "q00", "w51", "u71", "t00", "u70", "w71", "w70", "u60", "w60", "u61", "w61", "w40", "w31",
+    "w30", "w41", "u01", "w01", "u00", "w00",
 )
 RELAYED = (1, 2)
 DIRECT_OUT = (0, 3, 4)
-DIRECT_BACK = (0, 3, 4, 5, 6, 7)
+DIRECT_BACK = (0, 5, 6, 7)
 PLANES = tuple(p for p in range(8) if p not in RELAYED)
 FIRST_HALF = 0 if ORDER.index("a00") < ORDER.index("a01") else 1
 LAST_HALF = 1 if ORDER.index("w00") < ORDER.index("w01") else 0
@@ -76,7 +77,8 @@
             ids.at("br", p, r)
             for h in range(2):
                 for stage in ("ab", "ac", "rc", "rb"):
-                    ids.at(stage, p, h, r)
+                    if p not in RELAYED:
+                        ids.at(stage, p, h, r)
     for name in ("rz", "rzp", "gain"):
         ids.at(name)
     for p in RELAYED:
@@ -108,22 +110,22 @@
         c = core if c is None else c
         return (((z + dz) % NZ) * NX + (x + dx) % NX, ((y + dy) % NY) * 2 + c)
 
+    inputs = [
+        pltpu.make_async_copy(hidden_in, hidden_ref, isem.at[0]),
+        pltpu.make_async_copy(hidden_in.at[core], hbuf.at[core, 0, 0:BLK, 0:HALF], isem.at[1]),
+        pltpu.make_async_copy(gain_in, gbuf.at[tp], isem.at[2]),
+        pltpu.make_async_copy(eid_in, eid_ref, isem.at[3]),
+        pltpu.make_async_copy(rw_in, rw_ref, isem.at[4]),
+    ]
+    for cp in inputs:
+        cp.start()
+
     barrier = pltpu.get_barrier_semaphore()
     peers = [dev(dz=o, c=c) for o in range(1, NZ) for c in range(2)] + [dev(c=other)]
     peers += [dev(dy=o, c=c) for o in range(1, NY) for c in range(2)]
     peers += [dev(dx=o) for o in range(1, NX)]
     for peer in peers:
         pl.semaphore_signal(barrier, inc=1, device_id=peer, device_id_type=MESH)
-
-    inputs = [
-        pltpu.make_async_copy(eid_in, eid_ref, isem.at[0]),
-        pltpu.make_async_copy(rw_in, rw_ref, isem.at[1]),
-        pltpu.make_async_copy(hidden_in, hidden_ref, isem.at[2]),
-        pltpu.make_async_copy(hidden_in.at[core], hbuf.at[core, 0, 0:BLK, 0:HALF], isem.at[3]),
-        pltpu.make_async_copy(gain_in, gbuf.at[tp], isem.at[4]),
-    ]
-    for cp in inputs:
-        cp.start()
 
     def group(key):
         return GROUPS.index(key[0] + str(key[2]) if key[0] in RINGS + ("zs",) else key[0])
@@ -161,9 +163,6 @@
         weights.append((down_ref.at[e], wd.at[lanes(e * 256), :]))
     weights.append((sdown_ref, wsd.at[lanes(0), :]))
     local = [pltpu.make_async_copy(s, d, lsem.at[k]) for k, (s, d) in enumerate(weights)]
-    for cp in local:
-        cp.start()
-
     def live_slots(shape, dim):
         slot = lax.broadcasted_iota(jnp.int32, shape, dim)
         seq_len = jnp.zeros(shape, jnp.int32)
@@ -171,17 +170,11 @@
             seq_len = jnp.where(slot // 8 == q, len_ref[q], seq_len)
         return slot % 8 < seq_len
 
-    for cp in inputs:
-        cp.wait()
-    expert = lax.broadcasted_iota(jnp.int32, (128, 32), 0)
-    mix = jnp.zeros((128, 32), F32)
-    for k in range(8):
-        mix = mix + jnp.where(eid_ref[k : k + 1, :] == expert % 64, rw_ref[k : k + 1, :], 0.0)
-    mix = jnp.where(live_slots((128, 32), 1), mix, 0.0)
-    high = mix.astype(BF16).astype(F32)
-    terms = jnp.where(expert < 64, high, mix - high).T
-    rown[...] = terms.reshape(2, BLK, 128).astype(BF16)
-    rbuf[0, 0:BLK, :] = rown[core]
+    with jax.named_scope("inputs"):
+        for cp in inputs[:3]:
+            cp.wait()
+    for cp in local:
+        cp.start()
 
     with jax.named_scope("barrier"):
         pl.semaphore_wait(barrier, len(peers))
@@ -193,7 +186,6 @@
         if p not in RELAYED:
             for c in range(2):
                 push(hidden_ref.at[c], hbuf.at[core, p, 0:BLK, 0:HALF], ("z", p, 0), dev(dz=o, c=c), core)
-        push(rown.at[core], rbuf.at[p, 0:BLK, :], ("zr", p), dev(dz=o))
     for k, (s, d) in enumerate(weights):
         if k < 4:
             push(s, d, ("w", k), dev(c=other))
@@ -243,6 +235,21 @@
     def rslice(p, r):
         return rbuf.at[p, r * BLK : (r + 1) * BLK, :]
 
+    def route_start():
+        for cp in inputs[3:]:
+            cp.wait()
+        expert = lax.broadcasted_iota(jnp.int32, (128, 32), 0)
+        mix = jnp.zeros((128, 32), F32)
+        for k in range(8):
+            mix = mix + jnp.where(eid_ref[k : k + 1, :] == expert % 64, rw_ref[k : k + 1, :], 0.0)
+        mix = jnp.where(live_slots((128, 32), 1), mix, 0.0)
+        high = mix.astype(BF16).astype(F32)
+        terms = jnp.where(expert < 64, high, mix - high).T
+        rown[...] = terms.reshape(2, BLK, 128).astype(BF16)
+        rbuf[0, 0:BLK, :] = rown[core]
+        for o in range(1, NZ):
+            push(rown.at[core], rbuf.at[POS[-o % NZ], 0:BLK, :], ("zr", POS[-o % NZ]), dev(dz=o))
+
     def route_a(p):
         if p > 0:
             arrive(rslice(p, 0), ("zr", p))
@@ -318,15 +325,17 @@
     def silu(v):
         return v / (1.0 + jnp.exp(-v))
 
-    def normalise(g):
-        low, high = GROUPS_OF[g]
-        if g == 0:
+    firsts = {letter: next(n for n in ORDER if n[0] == letter) for letter in "nmv"}
+
+    def normalise(p):
+        g = next(k for k, planes in enumerate(GROUPS_OF) if p in planes)
+        offset = GROUPS_OF[g].index(p) * 64
+        if firsts["n"] == f"n{p}":
             arrive(gbuf.at[0:7], ("gain",))
 
         def block(b, carry):
-            p = low + (b // 4) * (high - low)
-            at = pl.ds(pl.multiple_of((b % 4) * BLK, BLK), BLK)
-            to = pl.ds(pl.multiple_of(b * BLK, BLK), BLK)
+            at = pl.ds(pl.multiple_of(b * BLK, BLK), BLK)
+            to = pl.ds(pl.multiple_of(offset + b * BLK, BLK), BLK)
             squares = jnp.zeros((BLK, HALF), F32)
             for h in range(2):
                 for r in range(NY):
@@ -337,30 +346,33 @@
                 for r in range(NY):
                     v = hbuf[h, p, at, r * HALF : (r + 1) * HALF].astype(F32)
                     gain = gbuf[((y + r) % NY) * 2 + h]
-                    hn[to, columns(h, r)] = (v * scale * gain).astype(BF16)
+                    hn[g, to, columns(h, r)] = (v * scale * gain).astype(BF16)
             return carry
 
-        lax.fori_loop(0, 8, block, 0)
-
-    def hidden_units(g):
-        if g == 0:
+        lax.fori_loop(0, 4, block, 0)
+
+    def hidden_units(g, e):
+        if firsts["m"] == f"m{g}{e}":
             weight_ready(range(0, 4))
         route = jnp.concatenate([rbuf[p] for p in GROUPS_OF[g]], axis=0)
         pick_row = lax.broadcasted_iota(jnp.int32, (128, 256), 0) % 64
-        for e in range(2):
-            pick = jnp.where(pick_row == ep * 2 + e, 1.0, 0.0).astype(BF16)
-            share = dot(route, pick)
-            gate = dot(hn[...], wgu[:, e * 256 : (e + 1) * 256])
-            up = dot(hn[...], wgu[:, 512 + e * 256 : 768 + e * 256])
-            inner[:, e * 256 : (e + 1) * 256] = (silu(gate) * up * share).astype(BF16)
-        if g == 0:
-            weight_ready(range(4, 9))
-            own = hn[0:BLK, :]
-            shared[...] = (silu(dot(own, wsgu[:, 0:256])) * dot(own, wsgu[:, 256:512])).astype(BF16)
+        pick = jnp.where(pick_row == ep * 2 + e, 1.0, 0.0).astype(BF16)
+        share = dot(route, pick)
+        gate = dot(hn[g], wgu[:, e * 256 : (e + 1) * 256])
+        up = dot(hn[g], wgu[:, 512 + e * 256 : 768 + e * 256])
+        inner[g, :, e * 256 : (e + 1) * 256] = (silu(gate) * up * share).astype(BF16)
+
+    def shared_units():
+        weight_ready(range(4, 6))
+        g = next(k for k, planes in enumerate(GROUPS_OF) if 0 in planes)
+        own = hn[g, 0:BLK, :]
+        shared[...] = (silu(dot(own, wsgu[:, 0:256])) * dot(own, wsgu[:, 256:512])).astype(BF16)
 
     def outputs(g, h):
+        if firsts["v"] == f"v{g}{h}":
+            weight_ready(range(6, 9))
         for r in range(NY):
-            part = dot(inner[...], wd[:, columns(h, r)])
+            part = dot(inner[g], wd[:, columns(h, r)])
             cols = slice(r * HALF, (r + 1) * HALF)
             for n, p in enumerate(GROUPS_OF[g]):
                 pbuf[h, p, :, cols] = part[n * 64 : (n + 1) * 64].astype(BF16)
@@ -437,8 +449,8 @@
             zb[0, core] = pbuf[core, 0, 0:BLK, 0:HALF]
             push(pbuf.at[other, 0, 0:BLK, 0:HALF], zb.at[0, core], ("rzp",), dev(c=other))
 
-    steps = dict(i=route_a, j=route_b, k=route_c, a=gather_a, b=gather_b, c=gather_c, d=gather_d, e=gather_e)
-    steps |= dict(n=normalise, m=hidden_units, v=outputs, q=relayed, r=sum_r, s=sum_s, t=sum_t, u=sum_u, w=sum_w)
+    steps = dict(y=route_start, i=route_a, j=route_b, k=route_c, a=gather_a, b=gather_b, c=gather_c, d=gather_d, e=gather_e)
+    steps |= dict(n=normalise, m=hidden_units, x=shared_units, v=outputs, q=relayed, r=sum_r, s=sum_s, t=sum_t, u=sum_u, w=sum_w)
     for name in ORDER:
         with jax.named_scope(name):
             steps[name[0]](*[int(digit) for digit in name[1:]])
@@ -472,7 +484,7 @@
 
 def body(hidden, norm_gain, expert_ids, route_weights, lengths, gate_proj, up_proj, down_proj, sgate, sup, sdown):
     vmem = pl.BlockSpec(memory_space=pltpu.VMEM)
-    anywhere = pl.BlockSpec(memory_space=pl.ANY)
+    anywhere = pl.BlockSpec(memory_space=pltpu.HBM)
     n = IDS.count
     out = pl.pallas_call(
         kernel,
@@ -485,8 +497,8 @@
             pltpu.VMEM((NZ, 64, 128), BF16),
             pltpu.VMEM((2, BLK, 128), BF16),
             pltpu.VMEM((8, 1, HALF), F32),
-            pltpu.VMEM((128, 4096), BF16),
-            pltpu.VMEM((128, 512), BF16),
+            pltpu.VMEM((4, 128, 4096), BF16),
+            pltpu.VMEM((4, 128, 512), BF16),
             pltpu.VMEM((BLK, 256), BF16),
             pltpu.VMEM((4096, 1024), BF16),
             pltpu.VMEM((512, 4096), BF16),

time: 67.9 us -> 67.7 us (level)
  no operation moved by 1% of the time
where the time goes in v4:
time: 67.7 us; the launch traced here: 67.4 us
  Pallas kernels  66.1 us (98%)
  local copies, waits for them, and re-layouts  1.38 us (2%)
    pallas_call x1, Pallas kernels, body(): pl.pallas_call(kernel, out_shape=jax.ShapeDtypeStruct((2, BLK, HALF), BF1...  66.1 us
    unnamed x1, local copies, waits for them, and re-layouts  1.38 us

profile of v4, /device:TPU:1, one launch (start us, length us, event | category | flops | bytes accessed | tf_op | source)
XLA Modules:
  0.0 67.4 jit_solution(15876476231812550393)
XLA Ops:
  0.0 66.1 %shard_map.109 = bf16[2,16,512]{2,1,0:T(8,128)(2,1)} custom-call(bf16[2,16,512]{2,1,0:T(8,128)(2,1)} %bitcast.6, f32[1,512]{1,0:T(1,128)} %bitcast.9, s32[8,32]{1,0:T(8,128)} %bitcast.7, f32[8,32]{1,0:T(8,128)} %bitcast.8, s32[4]{0:T(128)} %len_ref.1, bf16[2,4096,128]{2,1,0:T(8,128)(2,1)} %gate_ref.1, bf16[2,4096,128]{2,1,0:T(8,128)(2,1)} %up_ref.1, ...), custom_call_target="tpu_custom_call" | custom-call | tf_op jit(solution)/shard_map/pallas_call | solution.py:489
  66.1 1.4 %copy.13 = bf16[32,512]{1,0:T(8,128)(2,1)} copy(bf16[32,512]{1,0:T(8,128)(2,1)} %bitcast.5) | data formatting | bytes 65536

commit v5 on v4

--- a/solution.py
+++ b/solution.py
@@ -19,22 +19,22 @@
 
 GROUPS_OF = ((0, 3), (4, 5), (1, 2), (6, 7))
 ORDER = (
-    "a00", "a01", "y", "b01", "b00", "c00", "c01", "a31", "a30", "a50", "i5", "i2", "i4", "i3", "a41", "a40",
-    "a61", "a60", "a51", "i0", "i6", "i1", "d01", "a71", "a70", "b30", "d00", "i7", "b41", "b31", "c31", "c30",
-    "b51", "c41", "b50", "j6", "b71", "b70", "b40", "j3", "j4", "j7", "c40", "j5", "j2", "b60", "e01", "b61",
-    "e00", "n0", "j1", "d31", "d30", "j0", "c50", "c51", "c60", "k3", "k5", "d40", "c61", "x", "c70", "e11",
-    "k1", "k4", "e21", "d41", "k0", "c71", "k7", "k2", "k6", "e31", "e30", "n3", "m01", "m00", "d50", "d51",
-    "v00", "e10", "v01", "e20", "n1", "r31", "r30", "d60", "n2", "d61", "m21", "d70", "d71", "m20", "e40", "v21",
-    "v20", "e41", "e51", "e50", "n4", "n5", "m10", "s31", "m11", "v11", "r41", "v10", "r50", "r51", "e71", "e60",
-    "e61", "e70", "n7", "n6", "r40", "m30", "m31", "v31", "r71", "t31", "v30", "r70", "r61", "q11", "s41", "s50",
-    "s30", "r60", "s51", "q13", "s40", "q12", "s71", "r01", "q02", "q03", "s70", "r00", "s61", "u31", "s60", "t50",
-    "t41", "t51", "q01", "t30", "t40", "t71", "s01", "s00", "t70", "q10", "t60", "t61", "u40", "u41", "u51", "u50",
-    "w50", "u30", "t01", "q00", "w51", "u71", "t00", "u70", "w71", "w70", "u60", "w60", "u61", "w61", "w40", "w31",
-    "w30", "w41", "u01", "w01", "u00", "w00",
+    "a01", "a00", "y", "b01", "c01", "a31", "a30", "i1", "a51", "a40", "i0", "b00", "i3", "i2", "a60", "c00",
+    "a50", "a61", "a71", "d01", "b31", "a70", "j1", "i5", "i4", "b30", "b51", "a41", "i7", "c31", "c30", "b40",
+    "d00", "j5", "b71", "b50", "j0", "b61", "c51", "j2", "e01", "i6", "b41", "j7", "c40", "j3", "b60", "b70",
+    "d31", "k1", "c41", "d30", "k5", "j4", "e00", "c50", "c61", "n0", "x", "k7", "c71", "c60", "d40", "e11",
+    "e21", "j6", "k2", "k3", "c70", "k4", "e31", "k0", "d41", "d51", "e30", "n3", "m01", "m00", "d50", "v01",
+    "d61", "v00", "r31", "e10", "e20", "n2", "r30", "n1", "d60", "d71", "m20", "d70", "m21", "v21", "e51", "v20",
+    "e41", "k6", "e50", "n5", "e40", "e61", "n4", "m11", "s31", "s30", "m10", "v11", "r51", "v10", "e71", "r41",
+    "r50", "r40", "e70", "e60", "n6", "n7", "m30", "m31", "v30", "r70", "t30", "v31", "r71", "s51", "r60", "q13",
+    "r61", "s41", "q12", "s50", "s40", "q02", "q03", "s70", "r00", "s71", "r01", "q01", "s60", "s61", "q11", "t51",
+    "t31", "q10", "u30", "t50", "t41", "t40", "t70", "s00", "s01", "t71", "u31", "q00", "t60", "u51", "t61", "u50",
+    "u41", "u40", "u70", "t00", "t01", "u71", "w70", "w30", "w50", "w31", "w71", "w51", "w40", "u60", "w60", "u61",
+    "w61", "w41", "u00", "w00", "u01", "w01",
 )
 RELAYED = (1, 2)
 DIRECT_OUT = (0, 3, 4)
-DIRECT_BACK = (0, 5, 6, 7)
+DIRECT_BACK = (0, 6, 7)
 PLANES = tuple(p for p in range(8) if p not in RELAYED)
 FIRST_HALF = 0 if ORDER.index("a00") < ORDER.index("a01") else 1
 LAST_HALF = 1 if ORDER.index("w00") < ORDER.index("w01") else 0

time: 67.7 us -> 66.6 us (0.984)
  Pallas kernels: 66.1 us -> 65 us
    pallas_call x1, Pallas kernels: 66.1 us -> 65 us  [body(): pl.pallas_call(kernel, out_shape=jax.ShapeDtypeStruct((2, BLK, HALF), BF1...]
where the time goes in v5:
time: 66.6 us; the launch traced here: 66.4 us
  Pallas kernels  65 us (98%)
  local copies, waits for them, and re-layouts  1.38 us (2%)
    pallas_call x1, Pallas kernels, body(): pl.pallas_call(kernel, out_shape=jax.ShapeDtypeStruct((2, BLK, HALF), BF1...  65 us
    unnamed x1, local copies, waits for them, and re-layouts  1.38 us

profile of v5, /device:TPU:1, one launch (start us, length us, event | category | flops | bytes accessed | tf_op | source)
XLA Modules:
  0.0 66.4 jit_solution(6607355117776458724)
XLA Ops:
  0.0 65.0 %shard_map.109 = bf16[2,16,512]{2,1,0:T(8,128)(2,1)} custom-call(bf16[2,16,512]{2,1,0:T(8,128)(2,1)} %bitcast.6, f32[1,512]{1,0:T(1,128)} %bitcast.9, s32[8,32]{1,0:T(8,128)} %bitcast.7, f32[8,32]{1,0:T(8,128)} %bitcast.8, s32[4]{0:T(128)} %len_ref.1, bf16[2,4096,128]{2,1,0:T(8,128)(2,1)} %gate_ref.1, bf16[2,4096,128]{2,1,0:T(8,128)(2,1)} %up_ref.1, ...), custom_call_target="tpu_custom_call" | custom-call | tf_op jit(solution)/shard_map/pallas_call | solution.py:489
  65.0 1.4 %copy.13 = bf16[32,512]{1,0:T(8,128)(2,1)} copy(bf16[32,512]{1,0:T(8,128)(2,1)} %bitcast.5) | data formatting | bytes 65536
